TPU v7x, 512 devices: a whole 4x4x16 slice. The times are simulated.
512 devices in a mesh: sp: 128 (over z, x, core), tp: 4 (over y).
Axes of the slice: x: 4, y: 4, z: 16, core: 2. Of those that a mesh axis runs over, the one named last changes fastest.
Arguments:
- tokens: bfloat16 [65536, 2048], P(('sp', 'tp')), may hold values from -6 to 6
- input_norm_scale: bfloat16 [2048], replicated, may hold values from 0.099609375 to 1.8984375
- outer_gate_weight: bfloat16 [2048, 1024], P('sp', 'tp'), may hold values from -0.125 to 0.125
- inner_gate_weight: bfloat16 [2048, 1024], P('sp', 'tp'), may hold values from -0.125 to 0.125
- value_weight_matrix: bfloat16 [2048, 1024], P('sp', 'tp'), may hold values from -0.125 to 0.125
- output_gate_weight: bfloat16 [2048, 1024], P('sp', 'tp'), may hold values from -0.125 to 0.125
- state_input_weight: bfloat16 [2048, 1024], P('sp', 'tp'), may hold values from -0.125 to 0.125
- write_key_weight: bfloat16 [2048, 512], P('sp', 'tp'), may hold values from -0.125 to 0.125
- read_key_weight: bfloat16 [2048, 512], P('sp', 'tp'), may hold values from -0.125 to 0.125
- step_size_weight: bfloat16 [2048, 16], P(None, 'tp'), may hold values from -0.125 to 0.125
- gated_conv_weight: bfloat16 [3, 1024], P(None, 'tp'), may hold values from -3.5 to 3.5
- input_conv_weight: bfloat16 [4, 1024], P(None, 'tp'), may hold values from -3 to 3
- write_conv_weight: bfloat16 [4, 512], P(None, 'tp'), may hold values from -3 to 3
- read_conv_weight: bfloat16 [4, 512], P(None, 'tp'), may hold values from -3 to 3
- step_size_bias: float32 [16], P('tp'), may hold values from -1 to 0.5
- log_decay_rate: float32 [16], P('tp'), may hold values from -16 to -2.5, as said below
- decay_spikes: float32 [16, 65536], P('tp', 'sp'), may hold values from -1 to 0, as said below
- direct_path_weight: float32 [16], P('tp'), may hold values from 0.5 to 2
- head_norm_scale: bfloat16 [1024], P('tp'), may hold values from 0.099609375 to 1.8984375
- conv_output_weight: bfloat16 [1024, 2048], P('tp', 'sp'), may hold values from -0.125 to 0.125
- state_output_weight: bfloat16 [1024, 2048], P('tp', 'sp'), may hold values from -0.125 to 0.125
Outputs:
- mixed: bfloat16 [65536, 2048], P(('sp', 'tp'))
Inputs may be any that keep to these rules, and one draw needn't show every extreme that they name: `log_decay_rate`: one value a head. `decay_spikes`: never positive.
All inputs are finite; a program needn't handle non-finite values.
Results may differ from a plain program's by a relative error of at most 0.017.
Values may be sent and summed in bfloat16 or wider, within the bound.
A program may use at most 128 MiB of HBM per device.

v0:
```python
import jax
import jax.numpy as jnp
from jax import lax
from jax.sharding import Mesh
from jax.sharding import PartitionSpec as P

HEAD_DIM = 64
STATE = 128
BLOCK = 64
SP = ("sp_0", "sp_1", "sp_2")
SP_TP = ("sp_0", "sp_1", "sp_2", "tp")


epsilon = 1e-05


def in_order(tiles, dim):
    tiles = jnp.moveaxis(tiles, 0, dim)
    dims = tiles.shape
    return tiles.reshape(*dims[:dim], dims[dim] * dims[dim + 1], *dims[dim + 2 :])


def copy_for_each(shard, axis):
    devices = lax.axis_size(axis)
    return lax.all_to_all(
        jnp.broadcast_to(shard[None], (devices, *shard.shape)), axis, 0, 0, tiled=True
    )


def gather_directly(shard, axis, dim):
    return in_order(copy_for_each(shard, axis), dim)


def side_by_side(arrays, axis, dim, along):
    widths = [a.shape[along] for a in arrays]
    both = jnp.concatenate(arrays, axis=along)
    whole = lax.all_gather(both, axis, axis=dim, tiled=True)
    return tuple(jnp.split(whole, [sum(widths[:k]) for k in range(1, len(widths))], axis=along))


def shifted(shard, axis, by):
    devices = lax.axis_size(axis)
    pairs = [(i, i + by) for i in range(devices) if 0 <= i + by < devices]
    return lax.ppermute(shard, axis, pairs)


def filled_with(shard, identity):
    return jax.tree.map(
        lambda a, e: jnp.broadcast_to(jnp.asarray(e, a.dtype), a.shape), shard, identity
    )


def prefix_by_axis(shard, axes, combine, identity):
    before = start = filled_with(shard, identity)
    subtotal = shard
    for axis in reversed(axes):
        devices, index = (lax.axis_size(axis), lax.axis_index(axis))
        pieces = jax.tree.map(
            lambda part, kind: lax.all_gather(part.astype(kind), axis),
            subtotal,
            (jnp.bfloat16, jnp.bfloat16),
        )
        inside, subtotal = (start, start)
        for k in range(devices):
            passed = k < index
            subtotal = combine(
                subtotal, jax.tree.map(lambda part, own: part[k].astype(own.dtype), pieces, shard)
            )
            inside = jax.tree.map(lambda new, old: jnp.where(passed, new, old), subtotal, inside)
        before = combine(inside, before)
    return before


def whole_of(shard, axes, dim):
    far, near = axes
    tiles = copy_for_each(copy_for_each(shard, far), near)
    return in_order(tiles.swapaxes(0, 1).reshape(-1, *shard.shape), dim)


def side_by_side_2(arrays, axis, dim, along):
    both = jnp.concatenate(arrays, axis=along)
    whole, at, outs = (whole_of(both, axis, dim), 0, [])
    for a in arrays:
        outs.append(lax.slice_in_dim(whole, at, at + a.shape[along], axis=along))
        at += a.shape[along]
    return tuple(outs)


def split_up(shard, dim, devices):
    dims = shard.shape
    tiles = shard.reshape(*dims[:dim], devices, dims[dim] // devices, *dims[dim + 1 :])
    return jnp.moveaxis(tiles, dim, 0)


def summed_on_arrival(shard, axis, dim):
    tiles = split_up(shard, dim, lax.axis_size(axis))
    arrived = lax.all_to_all(tiles, axis, split_axis=0, concat_axis=0, tiled=True)
    return arrived.astype(jnp.float32).sum(axis=0)


def causal_taps(values, rim_rows, tap_weights):
    tap_count = tap_weights.shape[0]
    length = values.shape[0]
    padded = jnp.concatenate([rim_rows, values], axis=0)
    running = tap_weights[0] * padded[0:length]
    for offset in range(1, tap_count):
        running = running + tap_weights[offset] * padded[offset : offset + length]
    return running


def combine_states(earlier, later):
    return (earlier[0] * later[0], earlier[1] * later[0][:, None, None] + later[1])


def per_device(
    tokens,
    input_norm_scale,
    outer_gate_weight,
    inner_gate_weight,
    value_weight_matrix,
    output_gate_weight,
    state_input_weight,
    write_key_weight,
    read_key_weight,
    step_size_weight,
    gated_conv_weight,
    input_conv_weight,
    write_conv_weight,
    read_conv_weight,
    step_size_bias,
    log_decay_rate,
    decay_spikes,
    direct_path_weight,
    head_norm_scale,
    conv_output_weight,
    state_output_weight,
):
    token_rows = tokens.astype(jnp.float32)
    scaled = token_rows * lax.rsqrt(
        jnp.mean(token_rows * token_rows, axis=1, keepdims=True) + epsilon
    )
    normed_own = (scaled * input_norm_scale.astype(jnp.float32)).astype(jnp.bfloat16)
    normed = gather_directly(normed_own, "tp", 0)
    length = normed.shape[0]
    pieces = side_by_side(
        (
            outer_gate_weight,
            inner_gate_weight,
            value_weight_matrix,
            output_gate_weight,
            state_input_weight,
            write_key_weight,
            read_key_weight,
        ),
        SP,
        0,
        1,
    )
    projected = tuple(
        (jnp.dot(normed, weight_rows, preferred_element_type=jnp.float32) for weight_rows in pieces)
    )
    outer_gate, inner_gate, conv_input, out_gate, state_input, write_keys, read_keys = [
        member.astype(jnp.bfloat16) for member in projected
    ]
    step_raw = jnp.dot(normed, step_size_weight, preferred_element_type=jnp.float32)
    short_rim = gated_conv_weight.shape[0] - 1
    state_rim = input_conv_weight.shape[0] - 1
    rim_rows = shifted(
        (
            inner_gate[length - short_rim :],
            conv_input[length - short_rim :],
            state_input[length - state_rim :],
            write_keys[length - state_rim :],
            read_keys[length - state_rim :],
        ),
        SP,
        1,
    )
    product = inner_gate.astype(jnp.float32) * conv_input.astype(jnp.float32)
    rim_product = rim_rows[0].astype(jnp.float32) * rim_rows[1].astype(jnp.float32)
    mixer_part = (
        outer_gate.astype(jnp.float32)
        * causal_taps(product, rim_product, gated_conv_weight.astype(jnp.float32))
    ).astype(jnp.bfloat16)
    seq_input = jax.nn.silu(
        causal_taps(
            state_input.astype(jnp.float32),
            rim_rows[2].astype(jnp.float32),
            input_conv_weight.astype(jnp.float32),
        )
    )
    seq_write = jax.nn.silu(
        causal_taps(
            write_keys.astype(jnp.float32),
            rim_rows[3].astype(jnp.float32),
            write_conv_weight.astype(jnp.float32),
        )
    )
    seq_read = jax.nn.silu(
        causal_taps(
            read_keys.astype(jnp.float32),
            rim_rows[4].astype(jnp.float32),
            read_conv_weight.astype(jnp.float32),
        )
    )
    discrete_step = jax.nn.softplus(step_raw + step_size_bias[None, :])
    step_logarithm = discrete_step * (-jnp.exp(log_decay_rate))[None, :] + decay_spikes.T
    heads_here = discrete_step.shape[1]
    groups_here = seq_write.shape[1] // STATE
    per_group = heads_here // groups_here
    blocks = length // BLOCK
    input_blocks = seq_input.reshape(blocks, BLOCK, heads_here, HEAD_DIM)
    weighted = input_blocks * discrete_step.reshape(blocks, BLOCK, heads_here, 1)
    write_blocks = jnp.repeat(
        seq_write.reshape(blocks, BLOCK, groups_here, STATE), per_group, axis=2
    )
    read_blocks = jnp.repeat(seq_read.reshape(blocks, BLOCK, groups_here, STATE), per_group, axis=2)
    cumulative = jnp.cumsum(step_logarithm.reshape(blocks, BLOCK, heads_here), axis=1)
    causal = lax.broadcasted_iota(jnp.int32, (BLOCK, BLOCK), 0) >= lax.broadcasted_iota(
        jnp.int32, (BLOCK, BLOCK), 1
    )
    scores = jnp.einsum("clhm,cshm->clsh", read_blocks, write_blocks)
    damping = jnp.exp(
        jnp.where(
            causal[None, :, :, None],
            cumulative[:, :, None, :] - cumulative[:, None, :, :],
            -jnp.inf,
        )
    )
    within_block = jnp.einsum("clsh,cshp->clhp", scores * damping, weighted)
    to_end = jnp.exp(cumulative[:, -1:, :] - cumulative)
    block_states = jnp.einsum("cshm,cshp->chpm", write_blocks * to_end[..., None], weighted)
    block_logs = cumulative[:, -1, :]

    def advance(carried_state, inputs):
        contribution, block_log = inputs
        return (carried_state * jnp.exp(block_log)[:, None, None] + contribution, carried_state)

    own_total, own_before = lax.scan(
        advance, jnp.zeros(block_states.shape[1:], jnp.float32), (block_states, block_logs)
    )
    total_log = jnp.sum(block_logs, axis=0)
    arriving = prefix_by_axis(
        (jnp.exp(total_log), own_total),
        SP,
        combine_states,
        (jnp.ones_like(total_log), jnp.zeros_like(own_total)),
    )[1]
    before_logs = jnp.cumsum(block_logs, axis=0) - block_logs
    entering = own_before + jnp.exp(before_logs)[:, :, None, None] * arriving[None]
    from_before = (
        jnp.einsum("clhm,chpm->clhp", read_blocks, entering) * jnp.exp(cumulative)[..., None]
    )
    head_out = within_block + from_before + direct_path_weight[None, None, :, None] * input_blocks
    head_out = head_out.reshape(length, heads_here * HEAD_DIM)
    gated_heads = (head_out * jax.nn.silu(out_gate.astype(jnp.float32))).reshape(
        length, heads_here, HEAD_DIM
    )
    normalized = gated_heads * lax.rsqrt(
        jnp.mean(gated_heads * gated_heads, axis=2, keepdims=True) + epsilon
    )
    state_part = (
        normalized.reshape(length, heads_here * HEAD_DIM) * head_norm_scale.astype(jnp.float32)
    ).astype(jnp.bfloat16)
    wide_mixer, wide_state = side_by_side_2(
        (conv_output_weight, state_output_weight), (("sp_0", "sp_1"), "sp_2"), 1, 0
    )
    summed = summed_on_arrival(
        (
            jnp.dot(mixer_part, wide_mixer, preferred_element_type=jnp.float32)
            + jnp.dot(state_part, wide_state, preferred_element_type=jnp.float32)
        ).astype(jnp.bfloat16),
        "tp",
        0,
    )
    return summed.astype(jnp.bfloat16)


def solution(mesh):
    torus = Mesh(mesh.devices.reshape(16, 4, 2, mesh.shape["tp"]), ("sp_0", "sp_1", "sp_2", "tp"))
    return jax.shard_map(
        per_device,
        mesh=torus,
        in_specs=(
            P(SP_TP, None),
            P(),
            P(SP, "tp"),
            P(SP, "tp"),
            P(SP, "tp"),
            P(SP, "tp"),
            P(SP, "tp"),
            P(SP, "tp"),
            P(SP, "tp"),
            P(None, "tp"),
            P(None, "tp"),
            P(None, "tp"),
            P(None, "tp"),
            P(None, "tp"),
            P("tp"),
            P("tp"),
            P("tp", SP),
            P("tp"),
            P("tp"),
            P("tp", SP),
            P("tp", SP),
        ),
        out_specs=P(SP_TP, None),
        check_vma=False,
    )
```

profile of v0, /device:TPU:2, one launch (start us, length us, event | category | flops | bytes accessed | tf_op | source)
XLA Modules:
  0.0 331.9 jit_solution(838444194159853852)
XLA Ops:
  16.9 4.6 %all-to-all-start = ((bf16[4,128,2048]{2,1,0:T(8,128)(2,1)}), bf16[4,128,2048]{2,1,0:T(8,128)(2,1)S(1)}, u32[]{:S(2)}, u32[]{:S(2)}) async-start(bf16[4,128,2048]{2,1,0:T(8,128)(2,1)} %broadcast_in_dim.23), calls=%async_computation | async-start | bytes 4194304 | tf_op jit(solution)/shard_map/all_to_all | solution.py:25
  21.6 26.2 %all-to-all-done = bf16[4,128,2048]{2,1,0:T(8,128)(2,1)S(1)} async-done(((bf16[4,128,2048]{2,1,0:T(8,128)(2,1)}), bf16[4,128,2048]{2,1,0:T(8,128)(2,1)S(1)}, u32[]{:S(2)}, u32[]{:S(2)}) %all-to-all-start) | async-done | bytes 2097184 | tf_op jit(solution)/shard_map/all_to_all | solution.py:25
  48.9 18.6 %all-to-all-start.1 = ((bf16[64,512,16]{1,2,0:T(8,128)(2,1)}), bf16[64,512,16]{1,2,0:T(8,128)(2,1)S(1)}, u32[]{:S(2)}, u32[]{:S(2)}) async-start(bf16[64,512,16]{1,2,0:T(8,128)(2,1)} %broadcast_in_dim.24), calls=%async_computation.1 | async-start | bytes 2097152 | tf_op jit(solution)/shard_map/all_to_all | solution.py:25
  78.6 3.1 all-reduce
  83.8 8.2 %all-gather.2 = bf16[4,1,4]{2,1,0:T(2,128)(2,1)} all-gather(bf16[1,1,4]{2,1,0:T(2,128)(2,1)S(1)} %convert_bitcast_fusion), channel_id=1, replica_groups=mesh['sp_0'=16,'sp_1'=4,'sp_2'=2,'tp'=4] {'sp_1'}, dimensions={0}, use_global_device_ids=true | all-gather | bytes 40 | tf_op jit(solution)/shard_map/all_gather | solution.py:59
  104.5 34.2 %all-gather.3 = bf16[16,1,4]{2,1,0:T(2,128)(2,1)S(1)} all-gather(bf16[1,1,4]{2,1,0:T(2,128)(2,1)S(1)} %fusion.112), channel_id=1, replica_groups=mesh['sp_0'=16,'sp_1'=4,'sp_2'=2,'tp'=4] {'sp_0'}, dimensions={0}, use_global_device_ids=true | all-gather | bytes 136 | tf_op jit(solution)/shard_map/all_gather | solution.py:59
  144.0 5.5 %all_to_all.20 = bf16[2,64,512,16]{2,3,1,0:T(8,128)(2,1)S(1)} all-to-all(bf16[2,64,512,16]{2,3,1,0:T(8,128)(2,1)S(1)} %broadcast_in_dim.27), channel_id=1, replica_groups=mesh['sp_0'=16,'sp_1'=4,'sp_2'=2,'tp'=4] {'sp_2'}, dimensions={0} | all-to-all | bytes 4194304 | tf_op jit(solution)/shard_map/all_to_all | solution.py:25
  151.3 13.6 %all-gather.7.cloned.1.call-done = bf16[2048,1536]{1,0:T(8,128)(2,1)} async-done(((bf16[16,1536]{1,0:T(8,128)(2,1)}), bf16[2048,1536]{1,0:T(8,128)(2,1)}) %all-gather.7.cloned.1.call-update) | async-done | bytes 6291472 | tf_op jit(solution)/shard_map/all_gather | solution.py:37
  164.8 1.8 fusion.124
  166.7 2.1 collective-permute-start.3
  168.8 1.9 fusion.122
  170.8 3.2 collective-permute-start.2
  179.0 2.2 fusion.22
  181.2 18.8 %while.13 = (s32[]{:T(128)}, f32[4,64,128]{2,1,0:T(8,128)S(1)}, f32[8,4,64,128]{3,2,1,0:T(8,128)}, f32[8,4]{1,0:T(8,128)}, f32[8,4,64,128]{3,2,1,0:T(8,128)}, /*index=5*/s32[]{:T(128)}, s32[]{:T(128)}) while((s32[]{:T(128)}, f32[4,64,128]{2,1,0:T(8,128)S(1)}, f32[8,4,64,128]{3,2,1,0:T(8,128)}, f32[8,4]{1,0:T(8,128)}, ...), condition=%wide.region_3.4_spmd.clone, body=%wide.region_2.3_spmd.clone.sunk | while | flops 131075 | bytes 656016 | solution.py:239
  200.0 1.9 all-gather.1
  203.3 12.6 %all_gather.35 = bf16[4,4,64,128]{3,2,1,0:T(8,128)(2,1)S(1)} all-gather(bf16[1,4,64,128]{3,2,1,0:T(8,128)(2,1)S(1)} %fusion.92), channel_id=1, replica_groups=mesh['sp_0'=16,'sp_1'=4,'sp_2'=2,'tp'=4] {'sp_1'}, dimensions={0}, use_global_device_ids=true | all-gather | bytes 327680 | tf_op jit(solution)/shard_map/all_gather | solution.py:59
  218.1 1.7 fusion.123
  219.9 1.9 collective-permute-start.4
  221.8 1.9 convolution_convert_fusion.3
  223.8 2.7 convert_multiply_fusion.2
  226.5 1.9 collective-permute-start.1
  228.5 2.1 collective-permute-start
  231.4 1.9 collective-permute-done
  233.9 6.5 %fusion.10 = f32[512,2048]{1,0:T(8,128)} fusion(bf16[256,2048]{0,1:T(8,128)(2,1)} %bitcast.220, bf16[512,2048]{1,0:T(8,128)(2,1)S(1)} %bitcast.215, bf16[2048,1536]{1,0:T(8,128)(2,1)} %all-gather.7.cloned.1.call-done, f32[2,256]{1,0:T(2,128)} %convert_multiply_fusion.3, f32[512,256]{1,0:T(8,128)} %get-tuple-element.121, f32[256]{0:T(256)} %bitcast.230, ...), kind=kOutput, calls=%fused_computation.24 | convolution fusion | flops 1075183616 | bytes 8918016 | tf_op jit(solution)/shard_map/dot_general | solution.py:270
  240.4 2.3 convolution_bitcast_fusion.1
  242.7 44.7 %all-gather.9.cloned.1.call-done = bf16[16,4,64,128]{3,2,1,0:T(8,128)(2,1)} async-done(((bf16[1,4,64,128]{3,2,1,0:T(8,128)(2,1)}), bf16[16,4,64,128]{3,2,1,0:T(8,128)(2,1)}) %all-gather.9.cloned.1.call-update) | async-done | bytes 1048592 | tf_op jit(solution)/shard_map/all_gather | solution.py:59
  287.4 2.1 fusion.90
  289.5 2.7 fusion.5
  295.2 2.1 fusion.125
  298.5 2.9 add_convert_fusion
  301.5 20.7 %all_to_all.21 = bf16[4,128,2048]{2,1,0:T(8,128)(2,1)} all-to-all(bf16[4,128,2048]{2,1,0:T(8,128)(2,1)S(1)} %bitcast.217), channel_id=1, replica_groups=mesh['sp_0'=16,'sp_1'=4,'sp_2'=2,'tp'=4] {'tp'}, dimensions={0} | all-to-all | bytes 4194304 | tf_op jit(solution)/shard_map/all_to_all | solution.py:97
  322.2 2.9 reduce_sum.42
  (168 shorter events, 76.1 us)
Async XLA Ops:
  6.5 66.0 %copy-start = (bf16[2048,4]{0,1:T(4,128)(2,1)S(1)}, bf16[2048,4]{0,1:T(4,128)(2,1)}, u32[]{:S(2)}) copy-start(bf16[2048,4]{0,1:T(4,128)(2,1)} %param.32) | copy-start | bytes 49156
  6.5 158.3 %all-gather.7.cloned.1.call-start = ((), (), s32[]{:S(2)}) async-start(), calls=%async_computation.4 | async-start | bytes 6340608 | tf_op jit(solution)/shard_map/all_gather | solution.py:37
  16.9 4.6 %copy-start.8 = (bf16[256,16]{0,1:T(8,128)(2,1)S(1)}, bf16[256,16]{0,1:T(8,128)(2,1)}, u32[]{:S(2)}) copy-start(bf16[256,16]{0,1:T(8,128)(2,1)} %param.43) | copy-start | bytes 24580
  16.9 4.6 %copy-start.9 = (bf16[256,16]{0,1:T(8,128)(2,1)S(1)}, bf16[256,16]{0,1:T(8,128)(2,1)}, u32[]{:S(2)}) copy-start(bf16[256,16]{0,1:T(8,128)(2,1)} %param.42) | copy-start | bytes 24580
  16.9 30.9 %all-to-all-start = ((bf16[4,128,2048]{2,1,0:T(8,128)(2,1)}), bf16[4,128,2048]{2,1,0:T(8,128)(2,1)S(1)}, u32[]{:S(2)}, u32[]{:S(2)}) async-start(bf16[4,128,2048]{2,1,0:T(8,128)(2,1)} %broadcast_in_dim.23), calls=%async_computation | async-start | bytes 4194304 | tf_op jit(solution)/shard_map/all_to_all | solution.py:25
  21.5 46.7 %copy-start.24 = (bf16[4,128]{1,0:T(4,128)(2,1)S(1)}, bf16[4,128]{1,0:T(4,128)(2,1)}, u32[]{:S(2)}) copy-start(bf16[4,128]{1,0:T(4,128)(2,1)} %param.35) | copy-start | bytes 3076
  21.5 46.7 %copy-start.25 = (bf16[4,128]{1,0:T(4,128)(2,1)S(1)}, bf16[4,128]{1,0:T(4,128)(2,1)}, u32[]{:S(2)}) copy-start(bf16[4,128]{1,0:T(4,128)(2,1)} %param.36) | copy-start | bytes 3076
  21.5 48.6 %copy-start.27 = (f32[4]{0:T(128)S(1)}, f32[4]{0:T(128)}, u32[]{:S(2)}) copy-start(f32[4]{0:T(128)} %param.38) | copy-start | bytes 52
  21.5 49.8 %copy-start.10 = (bf16[3,256]{1,0:T(4,128)(2,1)S(1)}, bf16[3,256]{1,0:T(4,128)(2,1)}, u32[]{:S(2)}) copy-start(bf16[3,256]{1,0:T(4,128)(2,1)} %param.33) | copy-start | bytes 4612
  21.5 50.4 %copy-start.7 = (bf16[4,256]{1,0:T(4,128)(2,1)S(1)}, bf16[4,256]{1,0:T(4,128)(2,1)}, u32[]{:S(2)}) copy-start(bf16[4,256]{1,0:T(4,128)(2,1)} %param.34) | copy-start | bytes 6148
  21.6 51.0 %copy-start.6 = (f32[4,512]{1,0:T(4,128)S(1)}, f32[4,512]{1,0:T(4,128)}, u32[]{:S(2)}) copy-start(f32[4,512]{1,0:T(4,128)} %param.39) | copy-start | bytes 24580
  21.6 50.9 %copy-start.26 = (f32[4]{0:T(128)S(1)}, f32[4]{0:T(128)}, u32[]{:S(2)}) copy-start(f32[4]{0:T(128)} %param.37) | copy-start | bytes 52
  48.9 94.8 %all-to-all-start.1 = ((bf16[64,512,16]{1,2,0:T(8,128)(2,1)}), bf16[64,512,16]{1,2,0:T(8,128)(2,1)S(1)}, u32[]{:S(2)}, u32[]{:S(2)}) async-start(bf16[64,512,16]{1,2,0:T(8,128)(2,1)} %broadcast_in_dim.24), calls=%async_computation.1 | async-start | bytes 2097152 | tf_op jit(solution)/shard_map/all_to_all | solution.py:25
  67.6 219.8 %all-gather.9.cloned.1.call-start = ((), (), s32[]{:S(2)}) async-start(), calls=%async_computation.5 | async-start | bytes 1114112 | tf_op jit(solution)/shard_map/all_gather | solution.py:59
  166.6 7.5 %copy-start.19 = (f32[128]{0:T(128)S(1)}, f32[128]{0:T(128)}, u32[]{:S(2)}) copy-start(f32[128]{0:T(128)} %get-tuple-element.105) | copy-start | bytes 1540
  166.6 7.5 %copy-start.20 = (f32[128]{0:T(128)S(1)}, f32[128]{0:T(128)}, u32[]{:S(2)}) copy-start(f32[128]{0:T(128)} %get-tuple-element.106) | copy-start | bytes 1540
  166.6 7.5 %copy-start.21 = (f32[128]{0:T(128)S(1)}, f32[128]{0:T(128)}, u32[]{:S(2)}) copy-start(f32[128]{0:T(128)} %get-tuple-element.107) | copy-start | bytes 1540
  166.6 7.5 %copy-start.22 = (f32[128]{0:T(128)S(1)}, f32[128]{0:T(128)}, u32[]{:S(2)}) copy-start(f32[128]{0:T(128)} %get-tuple-element.108) | copy-start | bytes 1540
  166.6 9.1 %copy-start.11 = (f32[1,256]{1,0:T(1,128)S(1)}, f32[1,256]{1,0:T(1,128)}, u32[]{:S(2)}) copy-start(f32[1,256]{1,0:T(1,128)} %get-tuple-element.113) | copy-start | bytes 3076
  166.7 9.0 %copy-start.12 = (f32[1,256]{1,0:T(1,128)S(1)}, f32[1,256]{1,0:T(1,128)}, u32[]{:S(2)}) copy-start(f32[1,256]{1,0:T(1,128)} %get-tuple-element.114) | copy-start | bytes 3076
  166.7 9.0 %copy-start.13 = (f32[1,256]{1,0:T(1,128)S(1)}, f32[1,256]{1,0:T(1,128)}, u32[]{:S(2)}) copy-start(f32[1,256]{1,0:T(1,128)} %get-tuple-element.115) | copy-start | bytes 3076
  166.7 9.0 %copy-start.14 = (f32[1,256]{1,0:T(1,128)S(1)}, f32[1,256]{1,0:T(1,128)}, u32[]{:S(2)}) copy-start(f32[1,256]{1,0:T(1,128)} %get-tuple-element.116) | copy-start | bytes 3076
  166.7 7.3 %collective-permute-start.3 = (bf16[3,128]{1,0:T(4,128)(2,1)S(1)}, bf16[3,128]{1,0:T(4,128)(2,1)S(1)}, u32[]{:S(2)}, u32[]{:S(2)}) collective-permute-start(bf16[3,128]{1,0:T(4,128)(2,1)S(1)} %slice.362), channel_id=1, source_target_pairs={{0,4},{4,8},{8,12},{12,16},{16,20},{20,24},{24,28},{28,32},{32,36}... | collective-permute-start | bytes 2312 | tf_op jit(solution)/shard_map/ppermute | solution.py:44
  170.8 4.9 %collective-permute-start.2 = (bf16[3,256]{1,0:T(4,128)(2,1)S(1)}, bf16[3,256]{1,0:T(4,128)(2,1)S(1)}, u32[]{:S(2)}, u32[]{:S(2)}) collective-permute-start(bf16[3,256]{1,0:T(4,128)(2,1)S(1)} %slice.354), channel_id=1, source_target_pairs={{0,4},{4,8},{8,12},{12,16},{16,20},{20,24},{24,28},{28,32},{32,36}... | collective-permute-start | bytes 4616 | tf_op jit(solution)/shard_map/ppermute | solution.py:44
  219.9 10.7 %collective-permute-start.4 = (bf16[3,128]{1,0:T(4,128)(2,1)S(1)}, bf16[3,128]{1,0:T(4,128)(2,1)S(1)}, u32[]{:S(2)}, u32[]{:S(2)}) collective-permute-start(bf16[3,128]{1,0:T(4,128)(2,1)S(1)} %slice.367), channel_id=1, source_target_pairs={{0,4},{4,8},{8,12},{12,16},{16,20},{20,24},{24,28},{28,32},{32,36}... | collective-permute-start | bytes 2312 | tf_op jit(solution)/shard_map/ppermute | solution.py:44
  223.8 6.8 %copy-start.15 = (f32[128]{0:T(128)S(1)}, f32[128]{0:T(128)}, u32[]{:S(2)}) copy-start(f32[128]{0:T(128)} %get-tuple-element.109) | copy-start | bytes 1540
  223.8 6.8 %copy-start.16 = (f32[128]{0:T(128)S(1)}, f32[128]{0:T(128)}, u32[]{:S(2)}) copy-start(f32[128]{0:T(128)} %get-tuple-element.110) | copy-start | bytes 1540
  223.8 6.8 %copy-start.17 = (f32[128]{0:T(128)S(1)}, f32[128]{0:T(128)}, u32[]{:S(2)}) copy-start(f32[128]{0:T(128)} %get-tuple-element.111) | copy-start | bytes 1540
  223.8 6.8 %copy-start.18 = (f32[128]{0:T(128)S(1)}, f32[128]{0:T(128)}, u32[]{:S(2)}) copy-start(f32[128]{0:T(128)} %get-tuple-element.112) | copy-start | bytes 1540
  226.5 4.9 %collective-permute-start.1 = (bf16[2,256]{1,0:T(2,128)(2,1)S(1)}, bf16[2,256]{1,0:T(2,128)(2,1)S(1)}, u32[]{:S(2)}, u32[]{:S(2)}) collective-permute-start(bf16[2,256]{1,0:T(2,128)(2,1)S(1)} %slice.347), channel_id=1, source_target_pairs={{0,4},{4,8},{8,12},{12,16},{16,20},{20,24},{24,28},{28,32},{32,36}... | collective-permute-start | bytes 3080 | tf_op jit(solution)/shard_map/ppermute | solution.py:44
  228.5 4.9 %collective-permute-start = (bf16[2,256]{1,0:T(2,128)(2,1)S(1)}, bf16[2,256]{1,0:T(2,128)(2,1)S(1)}, u32[]{:S(2)}, u32[]{:S(2)}) collective-permute-start(bf16[2,256]{1,0:T(2,128)(2,1)S(1)} %slice.346), channel_id=1, source_target_pairs={{0,4},{4,8},{8,12},{12,16},{16,20},{20,24},{24,28},{28,32},{32,36}... | collective-permute-start | bytes 3080 | tf_op jit(solution)/shard_map/ppermute | solution.py:44
  287.4 2.1 copy-start.2
  (5 other events, 4.4 us)
Sparse Core Ops, SparseCore 0:
  12.2 152.5 all-gather.6
  218.2 69.1 all-gather.8
where the time goes:
time: 334 us; the launch traced here: 332 us
  waiting for transfers between devices  88.5 us (26%)
  blocking collectives  86.2 us (26%)
  local copies, waits for them, and re-layouts  39.4 us (12%)
  other arithmetic  38.3 us (11%)
  starting transfers between devices  34.6 us (10%)
  matrix products  30.1 us (9%)
  between operations  14.6 us (4%)
    all_gather x4, blocking collectives, prefix_by_axis(): lax.all_gather(part.astype(kind), axis)  56.9 us
    all_gather x1, waiting for transfers between devices, prefix_by_axis(): lax.all_gather(part.astype(kind), axis)  44.7 us
    all_to_all x2, waiting for transfers between devices, copy_for_each(): lax.all_to_all(jnp.broadcast_to(shard[None], (devices, *shard.shape)), ax...  26.2 us
    all_to_all x2, starting transfers between devices, copy_for_each(): lax.all_to_all(jnp.broadcast_to(shard[None], (devices, *shard.shape)), ax...  23.2 us
    all_to_all x1, blocking collectives, summed_on_arrival(): lax.all_to_all(tiles, axis, split_axis=0, concat_axis=0, tiled=True)  20.7 us
    all_gather x1, waiting for transfers between devices, side_by_side(): whole = lax.all_gather(both, axis, axis=dim, tiled=True)  13.6 us
    dot_general x6, matrix products, per_device(): jnp.dot(normed, weight_rows, preferred_element_type=jnp.float32)  12.2 us
    ppermute x5, starting transfers between devices, shifted(): return lax.ppermute(shard, axis, pairs)  11.3 us
  transfers between devices with their start and end apart: 9, of which 6 were waited for; matrix products, arithmetic and copies ran while one was open for 17% of the time, Pallas kernels for 0%

commit v1 on v0

v1 whole, which is shorter than its diff:
```python
import functools

import jax
import jax.numpy as jnp
from jax import lax
from jax.experimental import pallas as pl
from jax.experimental.pallas import tpu as pltpu
from jax.sharding import Mesh
from jax.sharding import PartitionSpec as P

SP = ("sp_0", "sp_1", "sp_2")
SP_TP = ("sp_0", "sp_1", "sp_2", "tp")
NZ, NX, NC, NY = 16, 4, 2, 4
PLANE = NX * NC
D = 2048
ROWS = 16
W = 256
STATE = 128
HEADS = 4
HEAD_DIM = 64
OWN = 128
LEN = 512
RIM = 16
L = 128
BLOCKS = LEN // L
NA = 5
GROUPS = 8
OUTER, INNER, VALUE, CONV_T, STATE_T, OUT_GATE, STATE_IN, KEYS = range(8)
EPS = 1e-05
MESH = pl.DeviceIdType.MESH
F32 = jnp.float32
BF16 = jnp.bfloat16
HIGH = lax.Precision.HIGHEST


def silu(v):
    return v / (1.0 + jnp.exp(-v))


def dot_nn(a, b, precision=None):
    return lax.dot_general(
        a, b, (((1,), (0,)), ((), ())), precision=precision, preferred_element_type=F32
    )


def dot_nt(a, b, precision=None):
    return lax.dot_general(
        a, b, (((1,), (1,)), ((), ())), precision=precision, preferred_element_type=F32
    )


def dot_tn(a, b, precision=None):
    return lax.dot_general(
        a, b, (((0,), (0,)), ((), ())), precision=precision, preferred_element_type=F32
    )


def iota(shape, dim):
    return lax.broadcasted_iota(jnp.int32, shape, dim)


def layer_kernel(
    tok,
    scale,
    outer_w,
    inner_w,
    value_w,
    out_gate_w,
    state_in_w,
    write_w,
    read_w,
    step_w,
    gated_taps,
    input_taps,
    write_taps,
    read_taps,
    bias,
    rate,
    spikes,
    direct,
    head_scale,
    conv_out_w,
    state_out_w,
    out,
    wbuf,
    nb,
    pj,
    product,
    mixer,
    spart,
    xin,
    wk,
    rk,
    within,
    cumx,
    before,
    decay,
    s_own,
    s1,
    pref,
    s2_own,
    s2,
    zin,
    s3_own,
    s3,
    t_own,
    t_plane,
    tz_own,
    t_z,
    rs_far,
    rs_right,
    rs_left,
    got_far_l,
    got_far_r,
    got_left,
    got_right,
    tok_s,
    tok_r,
    az_s,
    azl_r,
    azr_r,
    ax_s,
    axl_r,
    axr_r,
    axfl_r,
    axfr_r,
    bx_s,
    bx_r,
    bz_s,
    bzl_r,
    bzr_r,
    dd_s,
    dd_r,
    rim_s,
    rim_r,
    st_s,
    st_r,
    s2_s,
    s2_r,
    rs_s,
    rs_r,
):
    z = lax.axis_index("sp_0")
    x = lax.axis_index("sp_1")
    c = lax.axis_index("sp_2")
    y = lax.axis_index("tp")
    p = x * NC + c
    sp = z * PLANE + p

    def zm(k):
        return lax.rem(z + (k + NZ), NZ)

    def xm(k):
        return lax.rem(x + (k + NX), NX)

    def ym(k):
        return lax.rem(y + (k + NY), NY)

    def in_plane(k):
        q = lax.rem(p + k, PLANE)
        return q, (z, q // NC, lax.rem(q, NC), y)

    z_right, z_left = (zm(1), x, c, y), (zm(-1), x, c, y)
    x_right, x_left = (z, xm(1), c, y), (z, xm(-1), c, y)
    y_right, y_left = (z, x, c, ym(1)), (z, x, c, ym(-1))
    partner = (z, x, 1 - c, y)

    def along(k):
        q = lax.rem(sp + (k + NZ * PLANE), NZ * PLANE)
        r = lax.rem(q, PLANE)
        return (q // PLANE, r // NC, lax.rem(r, NC), y)

    barrier = pltpu.get_barrier_semaphore()

    def hello(where):
        pl.semaphore_signal(barrier, inc=1, device_id=where, device_id_type=MESH)

    hello(y_right)
    hello(y_left)
    hello(along(-1))

    def hello_plane(k, carry):
        hello(in_plane(k)[1])
        return carry

    def hello_z(k, carry):
        hello((lax.rem(z + k, NZ), x, c, y))
        return carry

    lax.fori_loop(1, PLANE, hello_plane, 0)
    lax.fori_loop(1, NZ, hello_z, 0)

    def send(src, dst, s_sem, r_sem, where):
        pltpu.make_async_remote_copy(
            src_ref=src,
            dst_ref=dst,
            send_sem=s_sem,
            recv_sem=r_sem,
            device_id=where,
            device_id_type=MESH,
        ).start()

    def wait(ref, sem):
        pltpu.make_async_copy(ref, ref, sem).wait()

    for group, ref in (
        (OUTER, outer_w),
        (INNER, inner_w),
        (VALUE, value_w),
        (OUT_GATE, out_gate_w),
        (STATE_IN, state_in_w),
    ):
        wbuf[group, z, x, c] = ref[...]
    wbuf[KEYS, z, x, c, :, 0:STATE] = write_w[...]
    wbuf[KEYS, z, x, c, :, STATE:W] = read_w[...]
    eye = (iota((W, W), 0) == iota((W, W), 1)).astype(BF16)
    wbuf[CONV_T, z, x, c] = dot_tn(conv_out_w[...], eye).astype(BF16)
    wbuf[STATE_T, z, x, c] = dot_tn(state_out_w[...], eye).astype(BF16)

    token_rows = tok[...].astype(F32)
    scaled = token_rows * lax.rsqrt(
        jnp.mean(token_rows * token_rows, axis=1, keepdims=True) + EPS
    )
    own_row = pl.multiple_of(RIM + y * OWN, RIM)
    nb[pl.ds(own_row, OWN)] = (scaled * scale[...].astype(F32)).astype(BF16)

    pl.semaphore_wait(barrier, 2 + 1 + (PLANE - 1) + (NZ - 1))

    HALF = OWN // 2

    def tok_piece(k, half):
        start = pl.multiple_of(RIM + ym(k) * OWN + half * HALF, RIM)
        return nb.at[pl.ds(start, HALF)]

    def send_tok(k, half, index, where):
        piece = tok_piece(k, half)
        send(piece, piece, tok_s.at[index], tok_r.at[index], where)

    def a_block(zz, xx):
        return wbuf.at[pl.ds(0, NA), zz, xx, c]

    def a_half(zz, xx, half):
        return wbuf.at[pl.ds(0, NA), zz, xx, c, :, pl.ds(half * 128, 128)]

    def b_block(xx):
        return wbuf.at[pl.ds(NA, GROUPS - NA), z, xx, c]

    def b_half(xx, half):
        return wbuf.at[pl.ds(NA, GROUPS - NA), z, xx, c, :, pl.ds(half * 128, 128)]

    def b_chunk(group, zz):
        return wbuf.at[group, zz, :, c]

    send(b_block(x), b_block(x), bx_s.at[0], bx_r.at[0], x_right)
    send(b_block(x), b_block(x), bx_s.at[1], bx_r.at[1], x_left)
    send_tok(0, 0, 0, y_right)
    send_tok(0, 1, 1, y_left)
    send_tok(0, 1, 2, y_right)
    send_tok(0, 0, 3, y_left)

    def az_send(k_right, k_left, step):
        if step <= 7:
            blk = a_block(zm(k_right), x)
            send(blk, blk, az_s, azl_r.at[step], z_right)
        if step <= 6:
            blk = a_block(zm(k_left), x)
            send(blk, blk, az_s, azr_r.at[step], z_left)

    def offsets(s):
        if s == 0:
            return [(0, 0)]
        found = [(-s, 0)]
        if s <= 7:
            found.append((s, 1))
        return found

    def ax_send(s):
        for k, side in offsets(s):
            i = 2 * s + side
            blk = a_block(zm(k), x)
            send(blk, blk, ax_s, axl_r.at[i], x_right)
            send(blk, blk, ax_s, axr_r.at[i], x_left)

    def ax_forward(s):
        for k, side in offsets(s):
            i = 2 * s + side
            wait(a_block(zm(k), xm(-1)), axl_r.at[i])
            half = a_half(zm(k), xm(-1), 0)
            send(half, half, ax_s, axfl_r.at[i], x_right)
            wait(a_block(zm(k), xm(1)), axr_r.at[i])
            half = a_half(zm(k), xm(1), 1)
            send(half, half, ax_s, axfr_r.at[i], x_left)

    def a_across(s):
        for k, side in offsets(s):
            i = 2 * s + side
            wait(a_half(zm(k), xm(2), 0), axfl_r.at[i])
            wait(a_half(zm(k), xm(2), 1), axfr_r.at[i])
            blk = wbuf.at[pl.ds(0, NA), zm(k), :, c]
            send(blk, blk, dd_s.at[0], dd_r.at[0], partner)

    def bz_send(k_right, k_left, step, group):
        b = group - NA
        if step <= 7:
            blk = b_chunk(group, zm(k_right))
            send(blk, blk, bz_s, bzl_r.at[b * 8 + step], z_right)
        if step <= 6:
            blk = b_chunk(group, zm(k_left))
            send(blk, blk, bz_s, bzr_r.at[b * 8 + step], z_left)

    def b_across(group, k):
        blk = b_chunk(group, zm(k))
        send(blk, blk, dd_s.at[1 + group - NA], dd_r.at[1 + group - NA], partner)

    order_b = (KEYS, STATE_IN, OUT_GATE)

    def b_round(s):
        for group in order_b:
            b = group - NA
            wait(b_chunk(group, zm(-s)), bzl_r.at[b * 8 + s - 1])
            if s <= 7:
                wait(b_chunk(group, zm(s)), bzr_r.at[b * 8 + s - 1])
            bz_send(-s, s, s, group)
            b_across(group, -s)
            if s <= 7:
                b_across(group, s)

    az_send(0, 0, 0)
    ax_send(0)
    wait(b_block(xm(-1)), bx_r.at[0])
    send(b_half(xm(-1), 0), b_half(xm(-1), 0), bx_s.at[2], bx_r.at[2], x_right)
    wait(b_block(xm(1)), bx_r.at[1])
    send(b_half(xm(1), 1), b_half(xm(1), 1), bx_s.at[3], bx_r.at[3], x_left)
    wait(b_half(xm(2), 0), bx_r.at[2])
    wait(b_half(xm(2), 1), bx_r.at[3])
    for group in order_b:
        bz_send(0, 0, 0, group)
    for group in order_b:
        b_across(group, 0)

    for s in range(1, 9):
        wait(a_block(zm(-s), x), azl_r.at[s - 1])
        if s <= 7:
            wait(a_block(zm(s), x), azr_r.at[s - 1])
        az_send(-s, s, s)
        ax_send(s)
        ax_forward(s - 1)
        if s >= 2:
            a_across(s - 2)
        b_round(s)
        if s == 2:
            wait(tok_piece(-1, 0), tok_r.at[0])
            send_tok(-1, 0, 4, y_right)
            wait(tok_piece(1, 1), tok_r.at[1])
            send_tok(1, 1, 5, y_left)
    ax_forward(8)
    a_across(7)

    wait(tok_piece(-1, 1), tok_r.at[2])
    wait(tok_piece(1, 0), tok_r.at[3])
    wait(tok_piece(2, 0), tok_r.at[4])
    wait(tok_piece(2, 1), tok_r.at[5])

    @pl.when(sp < NZ * PLANE - 1)
    def _():
        send(nb.at[pl.ds(LEN, RIM)], nb.at[pl.ds(0, RIM)], rim_s, rim_r, along(1))

    @pl.when(sp == 0)
    def _():
        nb[0:RIM] = jnp.zeros((RIM, D), BF16)

    step_raw = dot_nt(step_w[...], nb[RIM : RIM + LEN])
    head_row = iota((HEADS, LEN), 0)

    def per_head(ref, index):
        return functools.reduce(
            lambda got, h: jnp.where(index == h, ref[h], got),
            range(1, HEADS),
            jnp.full(index.shape, ref[0], F32),
        )

    shifted = step_raw + per_head(bias, head_row)
    step = jnp.maximum(shifted, 0.0) + jnp.log1p(jnp.exp(-jnp.abs(shifted)))
    log_step = step * (-jnp.exp(per_head(rate, head_row))) + spikes[...]
    ramp = (iota((L, L), 0) <= iota((L, L), 1)).astype(F32)
    spread = (iota((HEADS, W), 1) // HEAD_DIM == iota((HEADS, W), 0)).astype(F32)
    total = jnp.zeros((1, W), F32)
    cum_rows = []
    for b in range(BLOCKS):
        rows = dot_nn(log_step[:, b * L : (b + 1) * L], ramp, HIGH)
        cum_rows.append(rows)
        wide = dot_tn(rows, spread, HIGH)
        cumx[b] = wide
        decay[b] = wide[L - 1 : L]
        total = total + wide[L - 1 : L]
    t_own[0] = total

    for k in range(1, PLANE):
        _, where = in_plane(k)
        send(t_own, t_plane.at[pl.ds(p, 1)], st_s.at[0], st_r.at[0], where)
    t_plane[p] = total

    a_across(8)
    wait(t_plane.at[pl.ds(0, PLANE - 1)], st_r.at[0])
    tz_own[0] = jnp.sum(t_plane[...], axis=0)

    def send_tz(k, carry):
        there = lax.rem(z + k, NZ)
        send(tz_own, t_z.at[pl.ds(z, 1)], st_s.at[1], st_r.at[1], (there, x, c, y))
        return carry

    lax.fori_loop(1, NZ, send_tz, 0)

    @pl.when(sp > 0)
    def _():
        wait(nb.at[pl.ds(0, RIM)], rim_r)

    for b in range(GROUPS - NA):
        wait(wbuf.at[NA + b, :, :, 1 - c], dd_r.at[1 + b])

    def project(group, carry):
        acc = dot_nn(nb[...], wbuf[group].reshape(D, W))
        pj[group] = acc.astype(BF16).astype(F32)
        return carry

    lax.fori_loop(STATE_IN, KEYS + 1, project, 0)

    def causal(ref, taps, first, last):
        count = taps.shape[0]
        weights = taps[...].astype(F32)
        start = RIM - count + 1
        running = weights[0:1] * ref[start : start + LEN, first:last]
        for k in range(1, count):
            running = running + weights[k : k + 1] * ref[start + k : start + k + LEN, first:last]
        return running

    xin[...] = silu(causal(pj.at[STATE_IN], input_taps, 0, W))
    wk[...] = silu(causal(pj.at[KEYS], write_taps, 0, STATE)).astype(BF16)
    rk[...] = silu(causal(pj.at[KEYS], read_taps, STATE, W)).astype(BF16)

    state = jnp.zeros((STATE, W), F32)
    lane_head = iota((L, W), 1) // HEAD_DIM
    spread_l = (iota((HEADS, HEADS * L), 1) // L == iota((HEADS, HEADS * L), 0)).astype(F32)
    keep = iota((L, HEADS * L), 0) >= lax.rem(iota((L, HEADS * L), 1), L)
    weighted = []
    for b in range(BLOCKS):
        steps = dot_tn(step[:, b * L : (b + 1) * L], spread, HIGH)
        heavy = xin[b * L : (b + 1) * L] * steps
        weighted.append(heavy.astype(BF16))
        to_end = jnp.exp(decay[b] - cumx[b])
        own = dot_tn(wk[b * L : (b + 1) * L], (heavy * to_end).astype(BF16))
        before[b] = state
        state = state * jnp.exp(decay[b]) + own
    s_own[...] = state.astype(BF16).reshape(PLANE, ROWS, W)
    for k in range(1, PLANE):
        q, where = in_plane(k)
        send(s_own.at[q], s1.at[p], st_s.at[2], st_r.at[2], where)
    s1[p] = s_own[p]

    def within_block(b):
        rows = slice(b * L, (b + 1) * L)
        scores = dot_nt(rk[rows], wk[rows])
        cols = dot_tn(cum_rows[b], spread_l, HIGH)
        flat = jnp.concatenate([cum_rows[b][h : h + 1] for h in range(HEADS)], axis=1)
        damping = jnp.exp(jnp.where(keep, cols - flat, -jnp.inf))
        mixed = (jnp.concatenate([scores] * HEADS, axis=1) * damping).astype(BF16)
        stacked = jnp.concatenate(
            [jnp.where(lane_head == h, weighted[b], jnp.zeros_like(weighted[b])) for h in range(HEADS)],
            axis=0,
        )
        within[rows] = dot_nn(mixed, stacked)

    for b in range(BLOCKS):
        within_block(b)

    wait(s1.at[pl.ds(0, PLANE - 1)], st_r.at[2])
    running = jnp.zeros((ROWS, W), F32)
    for i in range(PLANE):
        pref[i] = running
        running = running * jnp.exp(t_plane[i]) + s1[i].astype(F32)
    s2_own[...] = running.astype(BF16)

    def send_s2(k, carry):
        @pl.when(z + k < NZ)
        def _():
            send(s2_own, s2.at[z], s2_s.at[k], s2_r.at[z], (z + k, x, c, y))

        return carry

    lax.fori_loop(1, NZ, send_s2, 0)

    wait(wbuf.at[pl.ds(0, NA), :, :, 1 - c], dd_r.at[0])
    lax.fori_loop(OUTER, VALUE + 1, project, 0)
    lax.fori_loop(OUT_GATE, OUT_GATE + 1, project, 0)
    product[...] = pj[INNER] * pj[VALUE]
    mixer[...] = (pj[OUTER, RIM : RIM + LEN] * causal(product, gated_taps, 0, W)).astype(BF16)

    wait(t_z.at[pl.ds(0, NZ - 1)], st_r.at[1])
    zin[...] = jnp.zeros((ROWS, W), F32)

    def take_s2(k, carry):
        @pl.when(k < z)
        def _():
            wait(s2.at[k], s2_r.at[k])
            zin[...] = zin[...] * jnp.exp(t_z[k]) + s2[k].astype(F32)

        return carry

    lax.fori_loop(0, NZ - 1, take_s2, 0)
    arriving = zin[...]
    logs = jnp.zeros((1, W), F32)
    for i in range(PLANE):
        s3_own[i] = (pref[i] + arriving * jnp.exp(logs)).astype(BF16)
        logs = logs + t_plane[i]
    for k in range(1, PLANE):
        q, where = in_plane(k)
        send(s3_own.at[q], s3.at[p], st_s.at[3], st_r.at[3], where)
    s3[p] = s3_own[p]

    lane = iota((1, W), 1) // HEAD_DIM
    direct_row = per_head(direct, lane)
    same_head = (iota((W, W), 0) // HEAD_DIM == iota((W, W), 1) // HEAD_DIM).astype(F32) * (
        1.0 / HEAD_DIM
    )
    gate = silu(pj[OUT_GATE, RIM : RIM + LEN])
    pj[OUT_GATE, RIM : RIM + LEN] = gate

    wait(s3.at[pl.ds(0, PLANE - 1)], st_r.at[3])
    entering = s3[...].reshape(STATE, W).astype(F32)
    logs = jnp.zeros((1, W), F32)
    for b in range(BLOCKS):
        rows = slice(b * L, (b + 1) * L)
        enter = (before[b] + jnp.exp(logs) * entering).astype(BF16)
        logs = logs + decay[b]
        head_out = (
            within[rows]
            + dot_nn(rk[rows], enter) * jnp.exp(cumx[b])
            + direct_row * xin[rows]
        )
        gated = head_out * pj[OUT_GATE, RIM + b * L : RIM + (b + 1) * L]
        mean = dot_nn(gated * gated, same_head, HIGH)
        spart[rows] = (gated * lax.rsqrt(mean + EPS) * head_scale[...].astype(F32)).astype(BF16)

    def partial(k):
        start = pl.multiple_of(ym(k) * OWN, OWN)
        return dot_nt(mixer[pl.ds(start, OWN)], wbuf[CONV_T].reshape(D, W)) + dot_nt(
            spart[pl.ds(start, OWN)], wbuf[STATE_T].reshape(D, W)
        )

    rs_far[...] = partial(2).astype(BF16)
    send(rs_far.at[0:HALF], got_far_l, rs_s.at[0], rs_r.at[0], y_right)
    send(rs_far.at[HALF:OWN], got_far_r, rs_s.at[1], rs_r.at[1], y_left)
    to_right = partial(1)
    rs_right[HALF:OWN] = to_right[HALF:OWN].astype(BF16)
    send(rs_right.at[HALF:OWN], got_left.at[HALF:OWN], rs_s.at[2], rs_r.at[2], y_right)
    to_left = partial(-1)
    rs_left[0:HALF] = to_left[0:HALF].astype(BF16)
    send(rs_left.at[0:HALF], got_right.at[0:HALF], rs_s.at[3], rs_r.at[3], y_left)
    wait(got_far_l, rs_r.at[0])
    rs_right[0:HALF] = (to_right[0:HALF] + got_far_l[...].astype(F32)).astype(BF16)
    send(rs_right.at[0:HALF], got_left.at[0:HALF], rs_s.at[4], rs_r.at[4], y_right)
    wait(got_far_r, rs_r.at[1])
    rs_left[HALF:OWN] = (to_left[HALF:OWN] + got_far_r[...].astype(F32)).astype(BF16)
    send(rs_left.at[HALF:OWN], got_right.at[HALF:OWN], rs_s.at[5], rs_r.at[5], y_left)
    mine = partial(0)

    for index, half in ((0, 0), (1, 1), (2, 1), (3, 0)):
        wait(tok_piece(0, half), tok_s.at[index])
    wait(tok_piece(-1, 0), tok_s.at[4])
    wait(tok_piece(1, 1), tok_s.at[5])
    wait(wbuf.at[pl.ds(0, NA), pl.ds(0, NZ - 1), 0, 0], az_s)
    wait(wbuf.at[pl.ds(0, NA), :, pl.ds(0, 3), 0], ax_s)
    wait(b_block(x), bx_s.at[0])
    wait(b_block(x), bx_s.at[1])
    wait(b_half(x, 0), bx_s.at[2])
    wait(b_half(x, 1), bx_s.at[3])
    wait(wbuf.at[pl.ds(NA, GROUPS - NA), pl.ds(0, NZ - 1), :, 0], bz_s)
    wait(wbuf.at[pl.ds(0, NA), :, :, c], dd_s.at[0])
    for b in range(GROUPS - NA):
        wait(wbuf.at[NA + b, :, :, c], dd_s.at[1 + b])

    @pl.when(sp < NZ * PLANE - 1)
    def _():
        wait(nb.at[pl.ds(LEN, RIM)], rim_s)

    wait(t_plane.at[pl.ds(0, PLANE - 1)], st_s.at[0])
    wait(t_z.at[pl.ds(0, NZ - 1)], st_s.at[1])
    wait(s_own.at[pl.ds(0, PLANE - 1)], st_s.at[2])
    wait(s3_own.at[pl.ds(0, PLANE - 1)], st_s.at[3])

    def left_s2(k, carry):
        @pl.when(z + k < NZ)
        def _():
            wait(s2_own, s2_s.at[k])

        return carry

    lax.fori_loop(1, NZ, left_s2, 0)
    wait(rs_far.at[0:HALF], rs_s.at[0])
    wait(rs_far.at[HALF:OWN], rs_s.at[1])
    wait(rs_right.at[HALF:OWN], rs_s.at[2])
    wait(rs_left.at[0:HALF], rs_s.at[3])
    wait(rs_right.at[0:HALF], rs_s.at[4])
    wait(rs_left.at[HALF:OWN], rs_s.at[5])

    wait(got_left.at[HALF:OWN], rs_r.at[2])
    wait(got_right.at[0:HALF], rs_r.at[3])
    wait(got_left.at[0:HALF], rs_r.at[4])
    wait(got_right.at[HALF:OWN], rs_r.at[5])
    out[...] = (mine + got_left[...].astype(F32) + got_right[...].astype(F32)).astype(BF16)


def per_device(
    tokens,
    input_norm_scale,
    outer_gate_weight,
    inner_gate_weight,
    value_weight_matrix,
    output_gate_weight,
    state_input_weight,
    write_key_weight,
    read_key_weight,
    step_size_weight,
    gated_conv_weight,
    input_conv_weight,
    write_conv_weight,
    read_conv_weight,
    step_size_bias,
    log_decay_rate,
    decay_spikes,
    direct_path_weight,
    head_norm_scale,
    conv_output_weight,
    state_output_weight,
):
    vmem = pl.BlockSpec(memory_space=pltpu.VMEM)
    smem = pl.BlockSpec(memory_space=pltpu.SMEM)
    dma = pltpu.SemaphoreType.DMA
    return pl.pallas_call(
        layer_kernel,
        out_shape=jax.ShapeDtypeStruct((OWN, D), BF16),
        in_specs=[vmem] * 14 + [smem, smem, vmem, smem] + [vmem] * 3,
        out_specs=vmem,
        scratch_shapes=[
            pltpu.VMEM((GROUPS, NZ, NX, NC, ROWS, W), BF16),
            pltpu.VMEM((RIM + LEN, D), BF16),
            pltpu.VMEM((GROUPS, RIM + LEN, W), F32),
            pltpu.VMEM((RIM + LEN, W), F32),
            pltpu.VMEM((LEN, W), BF16),
            pltpu.VMEM((LEN, W), BF16),
            pltpu.VMEM((LEN, W), F32),
            pltpu.VMEM((LEN, STATE), BF16),
            pltpu.VMEM((LEN, STATE), BF16),
            pltpu.VMEM((LEN, W), F32),
            pltpu.VMEM((BLOCKS, L, W), F32),
            pltpu.VMEM((BLOCKS, STATE, W), F32),
            pltpu.VMEM((BLOCKS, 1, W), F32),
            pltpu.VMEM((PLANE, ROWS, W), BF16),
            pltpu.VMEM((PLANE, ROWS, W), BF16),
            pltpu.VMEM((PLANE, ROWS, W), F32),
            pltpu.VMEM((ROWS, W), BF16),
            pltpu.VMEM((NZ, ROWS, W), BF16),
            pltpu.VMEM((ROWS, W), F32),
            pltpu.VMEM((PLANE, ROWS, W), BF16),
            pltpu.VMEM((PLANE, ROWS, W), BF16),
            pltpu.VMEM((1, 1, W), F32),
            pltpu.VMEM((PLANE, 1, W), F32),
            pltpu.VMEM((1, 1, W), F32),
            pltpu.VMEM((NZ, 1, W), F32),
            pltpu.VMEM((OWN, D), BF16),
            pltpu.VMEM((OWN, D), BF16),
            pltpu.VMEM((OWN, D), BF16),
            pltpu.VMEM((OWN // 2, D), BF16),
            pltpu.VMEM((OWN // 2, D), BF16),
            pltpu.VMEM((OWN, D), BF16),
            pltpu.VMEM((OWN, D), BF16),
            dma((6,)),
            dma((6,)),
            dma,
            dma((8,)),
            dma((8,)),
            dma,
            dma((18,)),
            dma((18,)),
            dma((18,)),
            dma((18,)),
            dma((4,)),
            dma((4,)),
            dma,
            dma((24,)),
            dma((24,)),
            dma((4,)),
            dma((4,)),
            dma,
            dma,
            dma((4,)),
            dma((4,)),
            dma((16,)),
            dma((16,)),
            dma((6,)),
            dma((6,)),
        ],
        compiler_params=pltpu.CompilerParams(
            collective_id=0, has_side_effects=True, vmem_limit_bytes=60 * 1024 * 1024
        ),
    )(
        tokens,
        input_norm_scale.reshape(1, D),
        outer_gate_weight,
        inner_gate_weight,
        value_weight_matrix,
        output_gate_weight,
        state_input_weight,
        write_key_weight,
        read_key_weight,
        step_size_weight.T,
        gated_conv_weight,
        input_conv_weight,
        write_conv_weight,
        read_conv_weight,
        step_size_bias,
        log_decay_rate,
        decay_spikes,
        direct_path_weight,
        head_norm_scale.reshape(1, W),
        conv_output_weight,
        state_output_weight,
    )


def solution(mesh):
    torus = Mesh(mesh.devices.reshape(NZ, NX, NC, mesh.shape["tp"]), SP_TP)
    return jax.shard_map(
        per_device,
        mesh=torus,
        in_specs=(
            P(SP_TP, None),
            P(),
            P(SP, "tp"),
            P(SP, "tp"),
            P(SP, "tp"),
            P(SP, "tp"),
            P(SP, "tp"),
            P(SP, "tp"),
            P(SP, "tp"),
            P(None, "tp"),
            P(None, "tp"),
            P(None, "tp"),
            P(None, "tp"),
            P(None, "tp"),
            P("tp"),
            P("tp"),
            P("tp", SP),
            P("tp"),
            P("tp"),
            P("tp", SP),
            P("tp", SP),
        ),
        out_specs=P(SP_TP, None),
        check_vma=False,
    )
```

time: 334 us -> 109 us (0.33)
  the two profiles are of different devices: /device:TPU:2 before, /device:TPU:1 now
where the time goes in v1:
time: 109 us
  Pallas kernels  103 us (94%)
  local copies, waits for them, and re-layouts  5.88 us (5%)
    pallas_call x1, Pallas kernels, per_device(): pl.pallas_call(layer_kernel, out_shape=jax.ShapeDtypeStruct((OWN, D), BF1...  103 us
    unnamed x7, local copies, waits for them, and re-layouts  3.35 us

profile of v1, /device:TPU:1, one launch (start us, length us, event | category | flops | bytes accessed | tf_op | source)
XLA Modules:
  0.0 108.9 jit_solution(15628424119443511217)
XLA Ops:
  0.0 0.0 copy-start
  0.0 1.3 %reshape.7.head_scale = bf16[1,256]{1,0:T(2,128)(2,1)} reshape(bf16[256]{0:T(256)(128)(2,1)} %param.39) | data formatting | bytes 1024 | tf_op jit(solution)/shard_map/reshape | solution.py:725
  1.3 1.3 %reshape.6.scale = bf16[1,2048]{1,0:T(2,128)(2,1)} reshape(bf16[2048]{0:T(1024)(128)(2,1)} %param.22) | data formatting | bytes 8192 | tf_op jit(solution)/shard_map/reshape | solution.py:708
  2.5 0.0 copy-done
  2.5 0.0 copy-start.1
  2.5 0.7 copy.22.conv_out_w
  3.3 0.0 copy-done.1
  3.3 0.7 copy.23.state_out_w
  4.0 103.0 %shard_map.199 = bf16[128,2048]{1,0:T(8,128)(2,1)} custom-call(bf16[128,2048]{1,0:T(8,128)(2,1)} %tok.1, bf16[1,2048]{1,0:T(2,128)(2,1)} %reshape.6.scale, bf16[16,256]{1,0:T(8,128)(2,1)} %outer_w.1, bf16[16,256]{1,0:T(8,128)(2,1)} %inner_w.1, bf16[16,256]{1,0:T(8,128)(2,1)} %value_w.1, bf16[16,256]{1,0:T(8,128)(2,1)} %out_gate_w.1, ...), custom_call_target="tpu_custom_call" | custom-call | tf_op jit(solution)/shard_map/pallas_call | solution.py:639
  107.0 1.9 %copy.25 = bf16[128,2048]{1,0:T(8,128)(2,1)} copy(bf16[128,2048]{1,0:T(8,128)(2,1)} %shard_map.199) | data formatting | bytes 1048576
Async XLA Ops:
  0.0 2.5 %copy-start = (bf16[256,16]{0,1:T(8,128)(2,1)S(1)}, bf16[256,16]{0,1:T(8,128)(2,1)}, u32[]{:S(2)}) copy-start(bf16[256,16]{0,1:T(8,128)(2,1)} %param.40) | copy-start | bytes 24580
  2.5 0.7 copy-start.1

commit v2 on v1

--- a/solution.py
+++ b/solution.py
@@ -60,8 +60,8 @@
 
 
 def layer_kernel(
-    tok,
-    scale,
+    tok_hbm,
+    scale_hbm,
     outer_w,
     inner_w,
     value_w,
@@ -69,6 +69,21 @@
     state_in_w,
     write_w,
     read_w,
+    step_w_hbm,
+    gated_taps_hbm,
+    input_taps_hbm,
+    write_taps_hbm,
+    read_taps_hbm,
+    bias_hbm,
+    rate_hbm,
+    spikes_hbm,
+    direct_hbm,
+    head_scale_hbm,
+    conv_out_w,
+    state_out_w,
+    out,
+    tok,
+    scale,
     step_w,
     gated_taps,
     input_taps,
@@ -79,15 +94,14 @@
     spikes,
     direct,
     head_scale,
-    conv_out_w,
-    state_out_w,
-    out,
+    in_s,
+    conv_part,
+    before_log,
     wbuf,
     nb,
     pj,
     product,
     mixer,
-    spart,
     xin,
     wk,
     rk,
@@ -170,6 +184,45 @@
         r = lax.rem(q, PLANE)
         return (q // PLANE, r // NC, lax.rem(r, NC), y)
 
+    weight_copies = [
+        pltpu.make_async_copy(ref, wbuf.at[group, z, x, c], in_s.at[group])
+        for group, ref in (
+            (OUTER, outer_w),
+            (INNER, inner_w),
+            (VALUE, value_w),
+            (CONV_T, conv_out_w),
+            (STATE_T, state_out_w),
+            (OUT_GATE, out_gate_w),
+            (STATE_IN, state_in_w),
+        )
+    ] + [
+        pltpu.make_async_copy(write_w, wbuf.at[KEYS, z, x, c, :, pl.ds(0, STATE)], in_s.at[7]),
+        pltpu.make_async_copy(read_w, wbuf.at[KEYS, z, x, c, :, pl.ds(STATE, STATE)], in_s.at[8]),
+    ]
+    token_copies = [
+        pltpu.make_async_copy(tok_hbm, tok, in_s.at[9]),
+        pltpu.make_async_copy(scale_hbm, scale, in_s.at[10]),
+    ]
+    small_copies = [
+        pltpu.make_async_copy(src, dst, in_s.at[11 + i])
+        for i, (src, dst) in enumerate(
+            (
+                (step_w_hbm, step_w),
+                (gated_taps_hbm, gated_taps),
+                (input_taps_hbm, input_taps),
+                (write_taps_hbm, write_taps),
+                (read_taps_hbm, read_taps),
+                (bias_hbm, bias),
+                (rate_hbm, rate),
+                (spikes_hbm, spikes),
+                (direct_hbm, direct),
+                (head_scale_hbm, head_scale),
+            )
+        )
+    ]
+    for copy in weight_copies + token_copies + small_copies:
+        copy.start()
+
     barrier = pltpu.get_barrier_semaphore()
 
     def hello(where):
@@ -203,29 +256,6 @@
     def wait(ref, sem):
         pltpu.make_async_copy(ref, ref, sem).wait()
 
-    for group, ref in (
-        (OUTER, outer_w),
-        (INNER, inner_w),
-        (VALUE, value_w),
-        (OUT_GATE, out_gate_w),
-        (STATE_IN, state_in_w),
-    ):
-        wbuf[group, z, x, c] = ref[...]
-    wbuf[KEYS, z, x, c, :, 0:STATE] = write_w[...]
-    wbuf[KEYS, z, x, c, :, STATE:W] = read_w[...]
-    eye = (iota((W, W), 0) == iota((W, W), 1)).astype(BF16)
-    wbuf[CONV_T, z, x, c] = dot_tn(conv_out_w[...], eye).astype(BF16)
-    wbuf[STATE_T, z, x, c] = dot_tn(state_out_w[...], eye).astype(BF16)
-
-    token_rows = tok[...].astype(F32)
-    scaled = token_rows * lax.rsqrt(
-        jnp.mean(token_rows * token_rows, axis=1, keepdims=True) + EPS
-    )
-    own_row = pl.multiple_of(RIM + y * OWN, RIM)
-    nb[pl.ds(own_row, OWN)] = (scaled * scale[...].astype(F32)).astype(BF16)
-
-    pl.semaphore_wait(barrier, 2 + 1 + (PLANE - 1) + (NZ - 1))
-
     HALF = OWN // 2
 
     def tok_piece(k, half):
@@ -245,18 +275,8 @@
     def b_block(xx):
         return wbuf.at[pl.ds(NA, GROUPS - NA), z, xx, c]
 
-    def b_half(xx, half):
-        return wbuf.at[pl.ds(NA, GROUPS - NA), z, xx, c, :, pl.ds(half * 128, 128)]
-
     def b_chunk(group, zz):
         return wbuf.at[group, zz, :, c]
-
-    send(b_block(x), b_block(x), bx_s.at[0], bx_r.at[0], x_right)
-    send(b_block(x), b_block(x), bx_s.at[1], bx_r.at[1], x_left)
-    send_tok(0, 0, 0, y_right)
-    send_tok(0, 1, 1, y_left)
-    send_tok(0, 1, 2, y_right)
-    send_tok(0, 0, 3, y_left)
 
     def az_send(k_right, k_left, step):
         if step <= 7:
@@ -321,40 +341,61 @@
             if s <= 7:
                 wait(b_chunk(group, zm(s)), bzr_r.at[b * 8 + s - 1])
             bz_send(-s, s, s, group)
+
+    def b_round_across(s):
+        for group in order_b:
             b_across(group, -s)
+            if 1 <= s <= 7:
+                b_across(group, s)
+
+    pl.semaphore_wait(barrier, 2 + 1 + (PLANE - 1) + (NZ - 1))
+    for copy in weight_copies:
+        copy.wait()
+    az_send(0, 0, 0)
+    for k in (1, 3, 2):
+        send(b_block(x), b_block(x), bx_s.at[k], bx_r.at[k], (z, xm(k), c, y))
+    ax_send(0)
+
+    for copy in token_copies:
+        copy.wait()
+    token_rows = tok[...].astype(F32)
+    scaled = token_rows * lax.rsqrt(
+        jnp.mean(token_rows * token_rows, axis=1, keepdims=True) + EPS
+    )
+    own_row = pl.multiple_of(RIM + y * OWN, RIM)
+    nb[pl.ds(own_row, OWN)] = (scaled * scale[...].astype(F32).reshape(1, D)).astype(BF16)
+    send_tok(0, 0, 0, y_right)
+    send_tok(0, 1, 1, y_left)
+    send_tok(0, 1, 2, y_right)
+    send_tok(0, 0, 3, y_left)
+
+    for s in range(1, 10):
+        if s <= 8:
+            wait(a_block(zm(-s), x), azl_r.at[s - 1])
             if s <= 7:
-                b_across(group, s)
-
-    az_send(0, 0, 0)
-    ax_send(0)
-    wait(b_block(xm(-1)), bx_r.at[0])
-    send(b_half(xm(-1), 0), b_half(xm(-1), 0), bx_s.at[2], bx_r.at[2], x_right)
-    wait(b_block(xm(1)), bx_r.at[1])
-    send(b_half(xm(1), 1), b_half(xm(1), 1), bx_s.at[3], bx_r.at[3], x_left)
-    wait(b_half(xm(2), 0), bx_r.at[2])
-    wait(b_half(xm(2), 1), bx_r.at[3])
-    for group in order_b:
-        bz_send(0, 0, 0, group)
-    for group in order_b:
-        b_across(group, 0)
-
-    for s in range(1, 9):
-        wait(a_block(zm(-s), x), azl_r.at[s - 1])
-        if s <= 7:
-            wait(a_block(zm(s), x), azr_r.at[s - 1])
-        az_send(-s, s, s)
-        ax_send(s)
-        ax_forward(s - 1)
+                wait(a_block(zm(s), x), azr_r.at[s - 1])
+            az_send(-s, s, s)
+            ax_send(s)
+        if s == 1:
+            for k in (1, 3, 2):
+                wait(b_block(xm(-k)), bx_r.at[k])
+            for group in order_b:
+                bz_send(0, 0, 0, group)
+        else:
+            b_round(s - 1)
         if s >= 2:
-            a_across(s - 2)
-        b_round(s)
-        if s == 2:
+            ax_forward(s - 2)
+            b_round_across(s - 2)
+        if s >= 4:
+            a_across(s - 4)
+        if s == 3:
             wait(tok_piece(-1, 0), tok_r.at[0])
             send_tok(-1, 0, 4, y_right)
             wait(tok_piece(1, 1), tok_r.at[1])
             send_tok(1, 1, 5, y_left)
+    b_round_across(8)
+    a_across(6)
     ax_forward(8)
-    a_across(7)
 
     wait(tok_piece(-1, 1), tok_r.at[2])
     wait(tok_piece(1, 0), tok_r.at[3])
@@ -368,6 +409,9 @@
     @pl.when(sp == 0)
     def _():
         nb[0:RIM] = jnp.zeros((RIM, D), BF16)
+
+    for copy in small_copies:
+        copy.wait()
 
     step_raw = dot_nt(step_w[...], nb[RIM : RIM + LEN])
     head_row = iota((HEADS, LEN), 0)
@@ -392,6 +436,7 @@
         wide = dot_tn(rows, spread, HIGH)
         cumx[b] = wide
         decay[b] = wide[L - 1 : L]
+        before_log[b] = total
         total = total + wide[L - 1 : L]
     t_own[0] = total
 
@@ -400,23 +445,14 @@
         send(t_own, t_plane.at[pl.ds(p, 1)], st_s.at[0], st_r.at[0], where)
     t_plane[p] = total
 
-    a_across(8)
-    wait(t_plane.at[pl.ds(0, PLANE - 1)], st_r.at[0])
-    tz_own[0] = jnp.sum(t_plane[...], axis=0)
-
-    def send_tz(k, carry):
-        there = lax.rem(z + k, NZ)
-        send(tz_own, t_z.at[pl.ds(z, 1)], st_s.at[1], st_r.at[1], (there, x, c, y))
-        return carry
-
-    lax.fori_loop(1, NZ, send_tz, 0)
+    a_across(7)
 
     @pl.when(sp > 0)
     def _():
         wait(nb.at[pl.ds(0, RIM)], rim_r)
 
-    for b in range(GROUPS - NA):
-        wait(wbuf.at[NA + b, :, :, 1 - c], dd_r.at[1 + b])
+    for group in (STATE_IN, KEYS):
+        wait(wbuf.at[group, :, :, 1 - c], dd_r.at[1 + group - NA])
 
     def project(group, carry):
         acc = dot_nn(nb[...], wbuf[group].reshape(D, W))
@@ -424,6 +460,7 @@
         return carry
 
     lax.fori_loop(STATE_IN, KEYS + 1, project, 0)
+    a_across(8)
 
     def causal(ref, taps, first, last):
         count = taps.shape[0]
@@ -457,6 +494,16 @@
         send(s_own.at[q], s1.at[p], st_s.at[2], st_r.at[2], where)
     s1[p] = s_own[p]
 
+    wait(t_plane.at[pl.ds(0, PLANE - 1)], st_r.at[0])
+    tz_own[0] = jnp.sum(t_plane[...], axis=0)
+
+    def send_tz(k, carry):
+        there = lax.rem(z + k, NZ)
+        send(tz_own, t_z.at[pl.ds(z, 1)], st_s.at[1], st_r.at[1], (there, x, c, y))
+        return carry
+
+    lax.fori_loop(1, NZ, send_tz, 0)
+
     def within_block(b):
         rows = slice(b * L, (b + 1) * L)
         scores = dot_nt(rk[rows], wk[rows])
@@ -489,11 +536,21 @@
 
     lax.fori_loop(1, NZ, send_s2, 0)
 
+    wait(wbuf.at[OUT_GATE, :, :, 1 - c], dd_r.at[1 + OUT_GATE - NA])
     wait(wbuf.at[pl.ds(0, NA), :, :, 1 - c], dd_r.at[0])
     lax.fori_loop(OUTER, VALUE + 1, project, 0)
     lax.fori_loop(OUT_GATE, OUT_GATE + 1, project, 0)
     product[...] = pj[INNER] * pj[VALUE]
     mixer[...] = (pj[OUTER, RIM : RIM + LEN] * causal(product, gated_taps, 0, W)).astype(BF16)
+
+    def conv_block(b, carry):
+        start = pl.multiple_of(b * OWN, OWN)
+        conv_part[pl.ds(start, OWN)] = dot_nt(
+            mixer[pl.ds(start, OWN)], wbuf[CONV_T].reshape(D, W)
+        )
+        return carry
+
+    lax.fori_loop(0, NY, conv_block, 0)
 
     wait(t_z.at[pl.ds(0, NZ - 1)], st_r.at[1])
     zin[...] = jnp.zeros((ROWS, W), F32)
@@ -527,25 +584,20 @@
 
     wait(s3.at[pl.ds(0, PLANE - 1)], st_r.at[3])
     entering = s3[...].reshape(STATE, W).astype(F32)
-    logs = jnp.zeros((1, W), F32)
-    for b in range(BLOCKS):
-        rows = slice(b * L, (b + 1) * L)
-        enter = (before[b] + jnp.exp(logs) * entering).astype(BF16)
-        logs = logs + decay[b]
+
+    def partial(k):
+        b = ym(k)
+        rows = pl.ds(pl.multiple_of(b * L, L), L)
+        enter = (before[b] + jnp.exp(before_log[b]) * entering).astype(BF16)
         head_out = (
             within[rows]
             + dot_nn(rk[rows], enter) * jnp.exp(cumx[b])
             + direct_row * xin[rows]
         )
-        gated = head_out * pj[OUT_GATE, RIM + b * L : RIM + (b + 1) * L]
+        gated = head_out * pj[OUT_GATE, pl.ds(pl.multiple_of(RIM + b * L, RIM), L)]
         mean = dot_nn(gated * gated, same_head, HIGH)
-        spart[rows] = (gated * lax.rsqrt(mean + EPS) * head_scale[...].astype(F32)).astype(BF16)
-
-    def partial(k):
-        start = pl.multiple_of(ym(k) * OWN, OWN)
-        return dot_nt(mixer[pl.ds(start, OWN)], wbuf[CONV_T].reshape(D, W)) + dot_nt(
-            spart[pl.ds(start, OWN)], wbuf[STATE_T].reshape(D, W)
-        )
+        part = (gated * lax.rsqrt(mean + EPS) * head_scale[...].astype(F32).reshape(1, W)).astype(BF16)
+        return conv_part[rows] + dot_nt(part, wbuf[STATE_T].reshape(D, W))
 
     rs_far[...] = partial(2).astype(BF16)
     send(rs_far.at[0:HALF], got_far_l, rs_s.at[0], rs_r.at[0], y_right)
@@ -570,10 +622,8 @@
     wait(tok_piece(1, 1), tok_s.at[5])
     wait(wbuf.at[pl.ds(0, NA), pl.ds(0, NZ - 1), 0, 0], az_s)
     wait(wbuf.at[pl.ds(0, NA), :, pl.ds(0, 3), 0], ax_s)
-    wait(b_block(x), bx_s.at[0])
-    wait(b_block(x), bx_s.at[1])
-    wait(b_half(x, 0), bx_s.at[2])
-    wait(b_half(x, 1), bx_s.at[3])
+    for k in (1, 2, 3):
+        wait(b_block(x), bx_s.at[k])
     wait(wbuf.at[pl.ds(NA, GROUPS - NA), pl.ds(0, NZ - 1), :, 0], bz_s)
     wait(wbuf.at[pl.ds(0, NA), :, :, c], dd_s.at[0])
     for b in range(GROUPS - NA):
@@ -634,19 +684,32 @@
     state_output_weight,
 ):
     vmem = pl.BlockSpec(memory_space=pltpu.VMEM)
-    smem = pl.BlockSpec(memory_space=pltpu.SMEM)
     dma = pltpu.SemaphoreType.DMA
     return pl.pallas_call(
         layer_kernel,
         out_shape=jax.ShapeDtypeStruct((OWN, D), BF16),
-        in_specs=[vmem] * 14 + [smem, smem, vmem, smem] + [vmem] * 3,
+        in_specs=[pl.BlockSpec(memory_space=pl.ANY)] * 21,
         out_specs=vmem,
         scratch_shapes=[
+            pltpu.VMEM((OWN, D), BF16),
+            pltpu.VMEM((D,), BF16),
+            pltpu.VMEM((HEADS, D), BF16),
+            pltpu.VMEM((3, W), BF16),
+            pltpu.VMEM((4, W), BF16),
+            pltpu.VMEM((4, STATE), BF16),
+            pltpu.VMEM((4, STATE), BF16),
+            pltpu.SMEM((HEADS,), F32),
+            pltpu.SMEM((HEADS,), F32),
+            pltpu.VMEM((HEADS, LEN), F32),
+            pltpu.SMEM((HEADS,), F32),
+            pltpu.VMEM((W,), BF16),
+            dma((21,)),
+            pltpu.VMEM((LEN, D), F32),
+            pltpu.VMEM((BLOCKS, 1, W), F32),
             pltpu.VMEM((GROUPS, NZ, NX, NC, ROWS, W), BF16),
             pltpu.VMEM((RIM + LEN, D), BF16),
             pltpu.VMEM((GROUPS, RIM + LEN, W), F32),
             pltpu.VMEM((RIM + LEN, W), F32),
-            pltpu.VMEM((LEN, W), BF16),
             pltpu.VMEM((LEN, W), BF16),
             pltpu.VMEM((LEN, W), F32),
             pltpu.VMEM((LEN, STATE), BF16),
@@ -705,7 +768,7 @@
         ),
     )(
         tokens,
-        input_norm_scale.reshape(1, D),
+        input_norm_scale,
         outer_gate_weight,
         inner_gate_weight,
         value_weight_matrix,
@@ -722,9 +785,9 @@
         log_decay_rate,
         decay_spikes,
         direct_path_weight,
-        head_norm_scale.reshape(1, W),
-        conv_output_weight,
-        state_output_weight,
+        head_norm_scale,
+        conv_output_weight.T,
+        state_output_weight.T,
     )
 
 

time: 109 us -> 97.6 us (0.90)
  Pallas kernels: 103 us -> 95.6 us
  local copies, waits for them, and re-layouts: 5.88 us -> 1.88 us
    pallas_call x1, Pallas kernels: 103 us -> 95.6 us  [per_device(): pl.pallas_call(layer_kernel, out_shape=jax.ShapeDtypeStruct((OWN, D), BF1...]
    reshape x2 -> x0, local copies, waits for them, and re-layouts: 2.54 us -> none  [the longest x1 1.28 us: per_device(): input_norm_scale.reshape(1, D)]
    unnamed x7 -> x1, local copies, waits for them, and re-layouts: 3.35 us -> 1.88 us
where the time goes in v2:
time: 97.6 us; the launch traced here: 97.5 us
  Pallas kernels  95.6 us (98%)
  local copies, waits for them, and re-layouts  1.88 us (2%)
    pallas_call x1, Pallas kernels, per_device(): pl.pallas_call(layer_kernel, out_shape=jax.ShapeDtypeStruct((OWN, D), BF1...  95.6 us

profile of v2, /device:TPU:1, one launch (start us, length us, event | category | flops | bytes accessed | tf_op | source)
XLA Modules:
  0.0 97.5 jit_solution(14588869551061847404)
XLA Ops:
  0.0 95.6 %shard_map.199 = bf16[128,2048]{1,0:T(8,128)(2,1)} custom-call(bf16[128,2048]{1,0:T(8,128)(2,1)} %tok_hbm.1, bf16[2048]{0:T(1024)(128)(2,1)} %scale_hbm.1, bf16[16,256]{1,0:T(8,128)(2,1)} %outer_w.1, bf16[16,256]{1,0:T(8,128)(2,1)} %inner_w.1, bf16[16,256]{1,0:T(8,128)(2,1)} %value_w.1, bf16[16,256]{1,0:T(8,128)(2,1)} %out_gate_w.1, ...), custom_call_target="tpu_custom_call" | custom-call | tf_op jit(solution)/shard_map/pallas_call | solution.py:688
  95.6 1.9 %copy.23 = bf16[128,2048]{1,0:T(8,128)(2,1)} copy(bf16[128,2048]{1,0:T(8,128)(2,1)} %shard_map.199) | data formatting | bytes 1048576

commit v3 on v2

--- a/solution.py
+++ b/solution.py
@@ -95,6 +95,7 @@
     direct,
     head_scale,
     in_s,
+    handed,
     conv_part,
     before_log,
     wbuf,
@@ -143,6 +144,8 @@
     bz_s,
     bzl_r,
     bzr_r,
+    pair_s,
+    pair_r,
     dd_s,
     dd_r,
     rim_s,
@@ -184,21 +187,24 @@
         r = lax.rem(q, PLANE)
         return (q // PLANE, r // NC, lax.rem(r, NC), y)
 
-    weight_copies = [
-        pltpu.make_async_copy(ref, wbuf.at[group, z, x, c], in_s.at[group])
-        for group, ref in (
-            (OUTER, outer_w),
-            (INNER, inner_w),
-            (VALUE, value_w),
-            (CONV_T, conv_out_w),
-            (STATE_T, state_out_w),
-            (OUT_GATE, out_gate_w),
-            (STATE_IN, state_in_w),
-        )
-    ] + [
-        pltpu.make_async_copy(write_w, wbuf.at[KEYS, z, x, c, :, pl.ds(0, STATE)], in_s.at[7]),
-        pltpu.make_async_copy(read_w, wbuf.at[KEYS, z, x, c, :, pl.ds(STATE, STATE)], in_s.at[8]),
-    ]
+    def weight_copies(whole):
+        return [
+            pltpu.make_async_copy(ref, whole.at[group], in_s.at[group])
+            for group, ref in (
+                (OUTER, outer_w),
+                (INNER, inner_w),
+                (VALUE, value_w),
+                (CONV_T, conv_out_w),
+                (STATE_T, state_out_w),
+                (OUT_GATE, out_gate_w),
+                (STATE_IN, state_in_w),
+            )
+        ] + [
+            pltpu.make_async_copy(write_w, whole.at[KEYS, :, pl.ds(0, STATE)], in_s.at[7]),
+            pltpu.make_async_copy(read_w, whole.at[KEYS, :, pl.ds(STATE, STATE)], in_s.at[8]),
+        ]
+
+    in_place = wbuf.at[:, z, x, 0]
     token_copies = [
         pltpu.make_async_copy(tok_hbm, tok, in_s.at[9]),
         pltpu.make_async_copy(scale_hbm, scale, in_s.at[10]),
@@ -220,7 +226,18 @@
             )
         )
     ]
-    for copy in weight_copies + token_copies + small_copies:
+
+    @pl.when(c == 0)
+    def _():
+        for copy in weight_copies(in_place):
+            copy.start()
+
+    @pl.when(c == 1)
+    def _():
+        for copy in weight_copies(handed):
+            copy.start()
+
+    for copy in token_copies + small_copies:
         copy.start()
 
     barrier = pltpu.get_barrier_semaphore()
@@ -232,16 +249,12 @@
     hello(y_left)
     hello(along(-1))
 
-    def hello_plane(k, carry):
-        hello(in_plane(k)[1])
-        return carry
-
-    def hello_z(k, carry):
-        hello((lax.rem(z + k, NZ), x, c, y))
-        return carry
-
-    lax.fori_loop(1, PLANE, hello_plane, 0)
-    lax.fori_loop(1, NZ, hello_z, 0)
+    hello(partner)
+
+    @pl.when(c == 0)
+    def _():
+        for where in (z_right, z_left, x_right, x_left, (z, xm(2), c, y)):
+            hello(where)
 
     def send(src, dst, s_sem, r_sem, where):
         pltpu.make_async_remote_copy(
@@ -267,16 +280,16 @@
         send(piece, piece, tok_s.at[index], tok_r.at[index], where)
 
     def a_block(zz, xx):
-        return wbuf.at[pl.ds(0, NA), zz, xx, c]
+        return wbuf.at[pl.ds(0, NA), zz, xx]
 
     def a_half(zz, xx, half):
-        return wbuf.at[pl.ds(0, NA), zz, xx, c, :, pl.ds(half * 128, 128)]
+        return wbuf.at[pl.ds(0, NA), zz, xx, half]
 
     def b_block(xx):
-        return wbuf.at[pl.ds(NA, GROUPS - NA), z, xx, c]
+        return wbuf.at[pl.ds(NA, GROUPS - NA), z, xx]
 
     def b_chunk(group, zz):
-        return wbuf.at[group, zz, :, c]
+        return wbuf.at[group, zz]
 
     def az_send(k_right, k_left, step):
         if step <= 7:
@@ -316,7 +329,7 @@
             i = 2 * s + side
             wait(a_half(zm(k), xm(2), 0), axfl_r.at[i])
             wait(a_half(zm(k), xm(2), 1), axfr_r.at[i])
-            blk = wbuf.at[pl.ds(0, NA), zm(k), :, c]
+            blk = wbuf.at[pl.ds(0, NA), zm(k)]
             send(blk, blk, dd_s.at[0], dd_r.at[0], partner)
 
     def bz_send(k_right, k_left, step, group):
@@ -348,13 +361,23 @@
             if 1 <= s <= 7:
                 b_across(group, s)
 
-    pl.semaphore_wait(barrier, 2 + 1 + (PLANE - 1) + (NZ - 1))
-    for copy in weight_copies:
-        copy.wait()
-    az_send(0, 0, 0)
-    for k in (1, 3, 2):
-        send(b_block(x), b_block(x), bx_s.at[k], bx_r.at[k], (z, xm(k), c, y))
-    ax_send(0)
+    @pl.when(c == 1)
+    def _():
+        pl.semaphore_wait(barrier, 4)
+        for copy in weight_copies(handed):
+            copy.wait()
+        send(handed, wbuf.at[:, z, x, 1], pair_s, pair_r, partner)
+
+    @pl.when(c == 0)
+    def _():
+        pl.semaphore_wait(barrier, 9)
+        for copy in weight_copies(in_place):
+            copy.wait()
+        wait(wbuf.at[:, z, x, 1], pair_r)
+        az_send(0, 0, 0)
+        for k in (1, 3, 2):
+            send(b_block(x), b_block(x), bx_s.at[k], bx_r.at[k], (z, xm(k), c, y))
+        ax_send(0)
 
     for copy in token_copies:
         copy.wait()
@@ -369,33 +392,42 @@
     send_tok(0, 1, 2, y_right)
     send_tok(0, 0, 3, y_left)
 
-    for s in range(1, 10):
-        if s <= 8:
-            wait(a_block(zm(-s), x), azl_r.at[s - 1])
-            if s <= 7:
-                wait(a_block(zm(s), x), azr_r.at[s - 1])
-            az_send(-s, s, s)
-            ax_send(s)
-        if s == 1:
-            for k in (1, 3, 2):
-                wait(b_block(xm(-k)), bx_r.at[k])
-            for group in order_b:
-                bz_send(0, 0, 0, group)
-        else:
-            b_round(s - 1)
-        if s >= 2:
-            ax_forward(s - 2)
-            b_round_across(s - 2)
-        if s >= 4:
-            a_across(s - 4)
-        if s == 3:
-            wait(tok_piece(-1, 0), tok_r.at[0])
-            send_tok(-1, 0, 4, y_right)
-            wait(tok_piece(1, 1), tok_r.at[1])
-            send_tok(1, 1, 5, y_left)
-    b_round_across(8)
-    a_across(6)
-    ax_forward(8)
+    def pass_tokens():
+        wait(tok_piece(-1, 0), tok_r.at[0])
+        send_tok(-1, 0, 4, y_right)
+        wait(tok_piece(1, 1), tok_r.at[1])
+        send_tok(1, 1, 5, y_left)
+
+    @pl.when(c == 1)
+    def _():
+        pass_tokens()
+
+    @pl.when(c == 0)
+    def _():
+        for s in range(1, 10):
+            if s <= 8:
+                wait(a_block(zm(-s), x), azl_r.at[s - 1])
+                if s <= 7:
+                    wait(a_block(zm(s), x), azr_r.at[s - 1])
+                az_send(-s, s, s)
+                ax_send(s)
+            if s == 1:
+                for k in (1, 3, 2):
+                    wait(b_block(xm(-k)), bx_r.at[k])
+                for group in order_b:
+                    bz_send(0, 0, 0, group)
+            else:
+                b_round(s - 1)
+            if s >= 2:
+                ax_forward(s - 2)
+                b_round_across(s - 2)
+            if s >= 4:
+                a_across(s - 4)
+            if s == 4:
+                pass_tokens()
+        b_round_across(8)
+        a_across(6)
+        ax_forward(8)
 
     wait(tok_piece(-1, 1), tok_r.at[2])
     wait(tok_piece(1, 0), tok_r.at[3])
@@ -440,19 +472,24 @@
         total = total + wide[L - 1 : L]
     t_own[0] = total
 
+    @pl.when(c == 0)
+    def _():
+        a_across(7)
+
+    @pl.when(sp > 0)
+    def _():
+        wait(nb.at[pl.ds(0, RIM)], rim_r)
+
+    @pl.when(c == 1)
+    def _():
+        for group in (STATE_IN, KEYS):
+            wait(wbuf.at[group], dd_r.at[1 + group - NA])
+
     for k in range(1, PLANE):
         _, where = in_plane(k)
         send(t_own, t_plane.at[pl.ds(p, 1)], st_s.at[0], st_r.at[0], where)
     t_plane[p] = total
 
-    a_across(7)
-
-    @pl.when(sp > 0)
-    def _():
-        wait(nb.at[pl.ds(0, RIM)], rim_r)
-
-    for group in (STATE_IN, KEYS):
-        wait(wbuf.at[group, :, :, 1 - c], dd_r.at[1 + group - NA])
 
     def project(group, carry):
         acc = dot_nn(nb[...], wbuf[group].reshape(D, W))
@@ -460,7 +497,11 @@
         return carry
 
     lax.fori_loop(STATE_IN, KEYS + 1, project, 0)
-    a_across(8)
+
+    @pl.when(c == 0)
+    def _():
+        a_across(8)
+
 
     def causal(ref, taps, first, last):
         count = taps.shape[0]
@@ -536,8 +577,11 @@
 
     lax.fori_loop(1, NZ, send_s2, 0)
 
-    wait(wbuf.at[OUT_GATE, :, :, 1 - c], dd_r.at[1 + OUT_GATE - NA])
-    wait(wbuf.at[pl.ds(0, NA), :, :, 1 - c], dd_r.at[0])
+    @pl.when(c == 1)
+    def _():
+        wait(wbuf.at[OUT_GATE], dd_r.at[1 + OUT_GATE - NA])
+        wait(wbuf.at[pl.ds(0, NA)], dd_r.at[0])
+
     lax.fori_loop(OUTER, VALUE + 1, project, 0)
     lax.fori_loop(OUT_GATE, OUT_GATE + 1, project, 0)
     product[...] = pj[INNER] * pj[VALUE]
@@ -614,20 +658,27 @@
     wait(got_far_r, rs_r.at[1])
     rs_left[HALF:OWN] = (to_left[HALF:OWN] + got_far_r[...].astype(F32)).astype(BF16)
     send(rs_left.at[HALF:OWN], got_right.at[HALF:OWN], rs_s.at[5], rs_r.at[5], y_left)
-    mine = partial(0)
+    own_sum = partial(0)
 
     for index, half in ((0, 0), (1, 1), (2, 1), (3, 0)):
         wait(tok_piece(0, half), tok_s.at[index])
     wait(tok_piece(-1, 0), tok_s.at[4])
     wait(tok_piece(1, 1), tok_s.at[5])
-    wait(wbuf.at[pl.ds(0, NA), pl.ds(0, NZ - 1), 0, 0], az_s)
-    wait(wbuf.at[pl.ds(0, NA), :, pl.ds(0, 3), 0], ax_s)
-    for k in (1, 2, 3):
-        wait(b_block(x), bx_s.at[k])
-    wait(wbuf.at[pl.ds(NA, GROUPS - NA), pl.ds(0, NZ - 1), :, 0], bz_s)
-    wait(wbuf.at[pl.ds(0, NA), :, :, c], dd_s.at[0])
-    for b in range(GROUPS - NA):
-        wait(wbuf.at[NA + b, :, :, c], dd_s.at[1 + b])
+
+    @pl.when(c == 1)
+    def _():
+        wait(handed, pair_s)
+
+    @pl.when(c == 0)
+    def _():
+        wait(wbuf.at[pl.ds(0, NA), pl.ds(0, NZ - 1), 0], az_s)
+        wait(wbuf.at[pl.ds(0, NA), :, pl.ds(0, 3)], ax_s)
+        for k in (1, 2, 3):
+            wait(b_block(x), bx_s.at[k])
+        wait(wbuf.at[pl.ds(NA, GROUPS - NA), pl.ds(0, NZ - 1)], bz_s)
+        wait(wbuf.at[pl.ds(0, NA)], dd_s.at[0])
+        for b in range(GROUPS - NA):
+            wait(wbuf.at[NA + b], dd_s.at[1 + b])
 
     @pl.when(sp < NZ * PLANE - 1)
     def _():
@@ -657,7 +708,7 @@
     wait(got_right.at[0:HALF], rs_r.at[3])
     wait(got_left.at[0:HALF], rs_r.at[4])
     wait(got_right.at[HALF:OWN], rs_r.at[5])
-    out[...] = (mine + got_left[...].astype(F32) + got_right[...].astype(F32)).astype(BF16)
+    out[...] = (own_sum + got_left[...].astype(F32) + got_right[...].astype(F32)).astype(BF16)
 
 
 def per_device(
@@ -704,6 +755,7 @@
             pltpu.SMEM((HEADS,), F32),
             pltpu.VMEM((W,), BF16),
             dma((21,)),
+            pltpu.VMEM((GROUPS, ROWS, W), BF16),
             pltpu.VMEM((LEN, D), F32),
             pltpu.VMEM((BLOCKS, 1, W), F32),
             pltpu.VMEM((GROUPS, NZ, NX, NC, ROWS, W), BF16),
@@ -752,6 +804,8 @@
             dma,
             dma((24,)),
             dma((24,)),
+            dma,
+            dma,
             dma((4,)),
             dma((4,)),
             dma,

time: 97.6 us -> 97.3 us (level)
  no operation moved by 1% of the time
where the time goes in v3:
time: 97.3 us; the launch traced here: 97.2 us
  Pallas kernels  95.3 us (98%)
  local copies, waits for them, and re-layouts  1.88 us (2%)
    pallas_call x1, Pallas kernels, per_device(): pl.pallas_call(layer_kernel, out_shape=jax.ShapeDtypeStruct((OWN, D), BF1...  95.3 us

profile of v3, /device:TPU:1, one launch (start us, length us, event | category | flops | bytes accessed | tf_op | source)
XLA Modules:
  0.0 97.2 jit_solution(3153815984712095137)
XLA Ops:
  0.0 95.3 %shard_map.199 = bf16[128,2048]{1,0:T(8,128)(2,1)} custom-call(bf16[128,2048]{1,0:T(8,128)(2,1)} %tok_hbm.1, bf16[2048]{0:T(1024)(128)(2,1)} %scale_hbm.1, bf16[16,256]{1,0:T(8,128)(2,1)} %outer_w.1, bf16[16,256]{1,0:T(8,128)(2,1)} %inner_w.1, bf16[16,256]{1,0:T(8,128)(2,1)} %value_w.1, bf16[16,256]{1,0:T(8,128)(2,1)} %out_gate_w.1, ...), custom_call_target="tpu_custom_call" | custom-call | tf_op jit(solution)/shard_map/pallas_call | solution.py:739
  95.3 1.9 %copy.23 = bf16[128,2048]{1,0:T(8,128)(2,1)} copy(bf16[128,2048]{1,0:T(8,128)(2,1)} %shard_map.199) | data formatting | bytes 1048576

commit v4 on v2

--- a/solution.py
+++ b/solution.py
@@ -23,7 +23,8 @@
 RIM = 16
 L = 128
 BLOCKS = LEN // L
-NA = 5
+NA = 6
+HOP = 2
 GROUPS = 8
 OUTER, INNER, VALUE, CONV_T, STATE_T, OUT_GATE, STATE_IN, KEYS = range(8)
 EPS = 1e-05
@@ -176,6 +177,8 @@
 
     z_right, z_left = (zm(1), x, c, y), (zm(-1), x, c, y)
     x_right, x_left = (z, xm(1), c, y), (z, xm(-1), c, y)
+    z_far_right, z_far_left = (zm(HOP), x, c, y), (zm(-HOP), x, c, y)
+    x_across = (z, xm(2), c, y)
     y_right, y_left = (z, x, c, ym(1)), (z, x, c, ym(-1))
     partner = (z, x, 1 - c, y)
 
@@ -185,7 +188,7 @@
         return (q // PLANE, r // NC, lax.rem(r, NC), y)
 
     weight_copies = [
-        pltpu.make_async_copy(ref, wbuf.at[group, z, x, c], in_s.at[group])
+        pltpu.make_async_copy(ref, wbuf.at[z, x, c, group], in_s.at[group])
         for group, ref in (
             (OUTER, outer_w),
             (INNER, inner_w),
@@ -196,8 +199,8 @@
             (STATE_IN, state_in_w),
         )
     ] + [
-        pltpu.make_async_copy(write_w, wbuf.at[KEYS, z, x, c, :, pl.ds(0, STATE)], in_s.at[7]),
-        pltpu.make_async_copy(read_w, wbuf.at[KEYS, z, x, c, :, pl.ds(STATE, STATE)], in_s.at[8]),
+        pltpu.make_async_copy(write_w, wbuf.at[z, x, c, KEYS, :, pl.ds(0, STATE)], in_s.at[7]),
+        pltpu.make_async_copy(read_w, wbuf.at[z, x, c, KEYS, :, pl.ds(STATE, STATE)], in_s.at[8]),
     ]
     token_copies = [
         pltpu.make_async_copy(tok_hbm, tok, in_s.at[9]),
@@ -232,16 +235,9 @@
     hello(y_left)
     hello(along(-1))
 
-    def hello_plane(k, carry):
-        hello(in_plane(k)[1])
-        return carry
-
-    def hello_z(k, carry):
-        hello((lax.rem(z + k, NZ), x, c, y))
-        return carry
-
-    lax.fori_loop(1, PLANE, hello_plane, 0)
-    lax.fori_loop(1, NZ, hello_z, 0)
+    hello(partner)
+    for where in (z_right, z_left, z_far_right, z_far_left, x_right, x_left, x_across):
+        hello(where)
 
     def send(src, dst, s_sem, r_sem, where):
         pltpu.make_async_remote_copy(
@@ -267,91 +263,85 @@
         send(piece, piece, tok_s.at[index], tok_r.at[index], where)
 
     def a_block(zz, xx):
-        return wbuf.at[pl.ds(0, NA), zz, xx, c]
+        return wbuf.at[zz, xx, c, pl.ds(0, NA)]
 
     def a_half(zz, xx, half):
-        return wbuf.at[pl.ds(0, NA), zz, xx, c, :, pl.ds(half * 128, 128)]
+        return wbuf.at[zz, xx, c, pl.ds(half * (NA // 2), NA // 2)]
 
     def b_block(xx):
-        return wbuf.at[pl.ds(NA, GROUPS - NA), z, xx, c]
+        return wbuf.at[z, xx, c, pl.ds(NA, GROUPS - NA)]
 
     def b_chunk(group, zz):
-        return wbuf.at[group, zz, :, c]
-
-    def az_send(k_right, k_left, step):
-        if step <= 7:
-            blk = a_block(zm(k_right), x)
-            send(blk, blk, az_s, azl_r.at[step], z_right)
-        if step <= 6:
-            blk = a_block(zm(k_left), x)
-            send(blk, blk, az_s, azr_r.at[step], z_left)
-
-    def offsets(s):
-        if s == 0:
-            return [(0, 0)]
-        found = [(-s, 0)]
-        if s <= 7:
-            found.append((s, 1))
-        return found
-
-    def ax_send(s):
-        for k, side in offsets(s):
-            i = 2 * s + side
-            blk = a_block(zm(k), x)
-            send(blk, blk, ax_s, axl_r.at[i], x_right)
-            send(blk, blk, ax_s, axr_r.at[i], x_left)
-
-    def ax_forward(s):
-        for k, side in offsets(s):
-            i = 2 * s + side
+        return wbuf.at[zz, :, c, group]
+
+    def goes_right(d):
+        return d != HOP - 1 and d < NZ // 2
+
+    def goes_left(d):
+        return d != HOP - 1 and d < NZ // 2 - 1
+
+    def z_pass(blk, k, s_sem, l_sem, r_sem, base):
+        if k <= 0 and goes_right(-k):
+            send(blk, blk, s_sem, l_sem.at[base - k], z_right)
+        if k >= 0 and goes_left(k):
+            send(blk, blk, s_sem, r_sem.at[base + k], z_left)
+        if k == 0:
+            send(blk, blk, s_sem, l_sem.at[base + HOP - 1], z_far_right)
+            send(blk, blk, s_sem, r_sem.at[base + HOP - 1], z_far_left)
+
+    def z_wait(blk, k, l_sem, r_sem, base):
+        wait(blk, l_sem.at[base - k - 1] if k < 0 else r_sem.at[base + k - 1])
+
+    def az_pass(k):
+        z_pass(a_block(zm(k), x), k, az_s, azl_r, azr_r, 0)
+
+    def bz_pass(group, k):
+        z_pass(b_chunk(group, zm(k)), k, bz_s, bzl_r, bzr_r, (group - NA) * 8)
+
+    def ax_send(k):
+        i = k % NZ
+        blk = a_block(zm(k), x)
+        send(blk, blk, ax_s, axl_r.at[i], x_right)
+        send(blk, blk, ax_s, axr_r.at[i], x_left)
+
+    def ax_forward(k):
+        i = k % NZ
+        wait(a_block(zm(k), xm(-1)), axl_r.at[i])
+        half = a_half(zm(k), xm(-1), 0)
+        send(half, half, ax_s, axfl_r.at[i], x_right)
+        wait(a_block(zm(k), xm(1)), axr_r.at[i])
+        half = a_half(zm(k), xm(1), 1)
+        send(half, half, ax_s, axfr_r.at[i], x_left)
+
+    def a_across(k):
+        i = k % NZ
+        if k == LAST:
             wait(a_block(zm(k), xm(-1)), axl_r.at[i])
-            half = a_half(zm(k), xm(-1), 0)
-            send(half, half, ax_s, axfl_r.at[i], x_right)
             wait(a_block(zm(k), xm(1)), axr_r.at[i])
-            half = a_half(zm(k), xm(1), 1)
-            send(half, half, ax_s, axfr_r.at[i], x_left)
-
-    def a_across(s):
-        for k, side in offsets(s):
-            i = 2 * s + side
+            wait(a_block(zm(k), xm(2)), axfl_r.at[i])
+        else:
             wait(a_half(zm(k), xm(2), 0), axfl_r.at[i])
             wait(a_half(zm(k), xm(2), 1), axfr_r.at[i])
-            blk = wbuf.at[pl.ds(0, NA), zm(k), :, c]
-            send(blk, blk, dd_s.at[0], dd_r.at[0], partner)
-
-    def bz_send(k_right, k_left, step, group):
-        b = group - NA
-        if step <= 7:
-            blk = b_chunk(group, zm(k_right))
-            send(blk, blk, bz_s, bzl_r.at[b * 8 + step], z_right)
-        if step <= 6:
-            blk = b_chunk(group, zm(k_left))
-            send(blk, blk, bz_s, bzr_r.at[b * 8 + step], z_left)
+        blk = wbuf.at[zm(k), :, c, pl.ds(0, NA)]
+        send(blk, blk, dd_s.at[0], dd_r.at[0], partner)
 
     def b_across(group, k):
         blk = b_chunk(group, zm(k))
         send(blk, blk, dd_s.at[1 + group - NA], dd_r.at[1 + group - NA], partner)
 
-    order_b = (KEYS, STATE_IN, OUT_GATE)
-
-    def b_round(s):
-        for group in order_b:
-            b = group - NA
-            wait(b_chunk(group, zm(-s)), bzl_r.at[b * 8 + s - 1])
-            if s <= 7:
-                wait(b_chunk(group, zm(s)), bzr_r.at[b * 8 + s - 1])
-            bz_send(-s, s, s, group)
-
-    def b_round_across(s):
-        for group in order_b:
-            b_across(group, -s)
-            if 1 <= s <= 7:
-                b_across(group, s)
-
-    pl.semaphore_wait(barrier, 2 + 1 + (PLANE - 1) + (NZ - 1))
+    order_b = (KEYS, STATE_IN)
+    LAST = -(NZ // 2)
+    rounds = [((0,),)]
+    for r in range(1, max(HOP - 1, NZ // 2 - HOP + 1) + 1):
+        near = [(-r, r)] if r < HOP else []
+        d = r + HOP - 1
+        far = [(-d, d) if d < NZ // 2 else (-d,)] if d <= NZ // 2 else []
+        rounds.append(tuple(near + far))
+
+    pl.semaphore_wait(barrier, 11)
     for copy in weight_copies:
         copy.wait()
-    az_send(0, 0, 0)
+    az_pass(0)
     for k in (1, 3, 2):
         send(b_block(x), b_block(x), bx_s.at[k], bx_r.at[k], (z, xm(k), c, y))
     ax_send(0)
@@ -369,33 +359,45 @@
     send_tok(0, 1, 2, y_right)
     send_tok(0, 0, 3, y_left)
 
-    for s in range(1, 10):
-        if s <= 8:
-            wait(a_block(zm(-s), x), azl_r.at[s - 1])
-            if s <= 7:
-                wait(a_block(zm(s), x), azr_r.at[s - 1])
-            az_send(-s, s, s)
-            ax_send(s)
-        if s == 1:
-            for k in (1, 3, 2):
-                wait(b_block(xm(-k)), bx_r.at[k])
+    for k in (1, 3, 2):
+        wait(b_block(xm(-k)), bx_r.at[k])
+    for group in order_b:
+        bz_pass(group, 0)
+
+    for r in range(1, len(rounds)):
+        for pair in rounds[r]:
+            for k in pair:
+                z_wait(a_block(zm(k), x), k, azl_r, azr_r, 0)
+                az_pass(k)
+            for k in pair:
+                ax_send(k)
+                if k == LAST:
+                    blk = a_block(zm(k), x)
+                    send(blk, blk, ax_s, axfl_r.at[k % NZ], x_across)
             for group in order_b:
-                bz_send(0, 0, 0, group)
-        else:
-            b_round(s - 1)
-        if s >= 2:
-            ax_forward(s - 2)
-            b_round_across(s - 2)
-        if s >= 4:
-            a_across(s - 4)
-        if s == 3:
+                for k in pair:
+                    z_wait(b_chunk(group, zm(k)), k, bzl_r, bzr_r, (group - NA) * 8)
+                    bz_pass(group, k)
+        for pair in rounds[r - 1]:
+            for k in pair:
+                ax_forward(k)
+                for group in order_b:
+                    b_across(group, k)
+        if r >= 2:
+            for pair in rounds[r - 2]:
+                for k in pair:
+                    a_across(k)
+        if r == 2:
             wait(tok_piece(-1, 0), tok_r.at[0])
             send_tok(-1, 0, 4, y_right)
             wait(tok_piece(1, 1), tok_r.at[1])
             send_tok(1, 1, 5, y_left)
-    b_round_across(8)
-    a_across(6)
-    ax_forward(8)
+    for pair in rounds[-1]:
+        for k in pair:
+            for group in order_b:
+                b_across(group, k)
+            if k != LAST:
+                ax_forward(k)
 
     wait(tok_piece(-1, 1), tok_r.at[2])
     wait(tok_piece(1, 0), tok_r.at[3])
@@ -445,22 +447,26 @@
         send(t_own, t_plane.at[pl.ds(p, 1)], st_s.at[0], st_r.at[0], where)
     t_plane[p] = total
 
-    a_across(7)
+    for pair in rounds[-2]:
+        for k in pair:
+            a_across(k)
 
     @pl.when(sp > 0)
     def _():
         wait(nb.at[pl.ds(0, RIM)], rim_r)
 
     for group in (STATE_IN, KEYS):
-        wait(wbuf.at[group, :, :, 1 - c], dd_r.at[1 + group - NA])
+        wait(wbuf.at[:, :, 1 - c, group], dd_r.at[1 + group - NA])
 
     def project(group, carry):
-        acc = dot_nn(nb[...], wbuf[group].reshape(D, W))
+        acc = dot_nn(nb[...], wbuf[:, :, :, group].reshape(D, W))
         pj[group] = acc.astype(BF16).astype(F32)
         return carry
 
     lax.fori_loop(STATE_IN, KEYS + 1, project, 0)
-    a_across(8)
+    for pair in rounds[-1]:
+        for k in pair:
+            a_across(k)
 
     def causal(ref, taps, first, last):
         count = taps.shape[0]
@@ -536,8 +542,7 @@
 
     lax.fori_loop(1, NZ, send_s2, 0)
 
-    wait(wbuf.at[OUT_GATE, :, :, 1 - c], dd_r.at[1 + OUT_GATE - NA])
-    wait(wbuf.at[pl.ds(0, NA), :, :, 1 - c], dd_r.at[0])
+    wait(wbuf.at[:, :, 1 - c, pl.ds(0, NA)], dd_r.at[0])
     lax.fori_loop(OUTER, VALUE + 1, project, 0)
     lax.fori_loop(OUT_GATE, OUT_GATE + 1, project, 0)
     product[...] = pj[INNER] * pj[VALUE]
@@ -546,7 +551,7 @@
     def conv_block(b, carry):
         start = pl.multiple_of(b * OWN, OWN)
         conv_part[pl.ds(start, OWN)] = dot_nt(
-            mixer[pl.ds(start, OWN)], wbuf[CONV_T].reshape(D, W)
+            mixer[pl.ds(start, OWN)], wbuf[:, :, :, CONV_T].reshape(D, W)
         )
         return carry
 
@@ -597,7 +602,7 @@
         gated = head_out * pj[OUT_GATE, pl.ds(pl.multiple_of(RIM + b * L, RIM), L)]
         mean = dot_nn(gated * gated, same_head, HIGH)
         part = (gated * lax.rsqrt(mean + EPS) * head_scale[...].astype(F32).reshape(1, W)).astype(BF16)
-        return conv_part[rows] + dot_nt(part, wbuf[STATE_T].reshape(D, W))
+        return conv_part[rows] + dot_nt(part, wbuf[:, :, :, STATE_T].reshape(D, W))
 
     rs_far[...] = partial(2).astype(BF16)
     send(rs_far.at[0:HALF], got_far_l, rs_s.at[0], rs_r.at[0], y_right)
@@ -620,14 +625,14 @@
         wait(tok_piece(0, half), tok_s.at[index])
     wait(tok_piece(-1, 0), tok_s.at[4])
     wait(tok_piece(1, 1), tok_s.at[5])
-    wait(wbuf.at[pl.ds(0, NA), pl.ds(0, NZ - 1), 0, 0], az_s)
-    wait(wbuf.at[pl.ds(0, NA), :, pl.ds(0, 3), 0], ax_s)
+    wait(wbuf.at[pl.ds(0, NZ - 1), 0, 0, pl.ds(0, NA)], az_s)
+    wait(wbuf.at[:, pl.ds(0, 3), 0, pl.ds(0, NA)], ax_s)
     for k in (1, 2, 3):
         wait(b_block(x), bx_s.at[k])
-    wait(wbuf.at[pl.ds(NA, GROUPS - NA), pl.ds(0, NZ - 1), :, 0], bz_s)
-    wait(wbuf.at[pl.ds(0, NA), :, :, c], dd_s.at[0])
+    wait(wbuf.at[pl.ds(0, NZ - 1), :, 0, pl.ds(NA, GROUPS - NA)], bz_s)
+    wait(wbuf.at[:, :, c, pl.ds(0, NA)], dd_s.at[0])
     for b in range(GROUPS - NA):
-        wait(wbuf.at[NA + b, :, :, c], dd_s.at[1 + b])
+        wait(wbuf.at[:, :, c, NA + b], dd_s.at[1 + b])
 
     @pl.when(sp < NZ * PLANE - 1)
     def _():
@@ -706,7 +711,7 @@
             dma((21,)),
             pltpu.VMEM((LEN, D), F32),
             pltpu.VMEM((BLOCKS, 1, W), F32),
-            pltpu.VMEM((GROUPS, NZ, NX, NC, ROWS, W), BF16),
+            pltpu.VMEM((NZ, NX, NC, GROUPS, ROWS, W), BF16),
             pltpu.VMEM((RIM + LEN, D), BF16),
             pltpu.VMEM((GROUPS, RIM + LEN, W), F32),
             pltpu.VMEM((RIM + LEN, W), F32),
@@ -750,8 +755,8 @@
             dma((4,)),
             dma((4,)),
             dma,
-            dma((24,)),
-            dma((24,)),
+            dma((16,)),
+            dma((16,)),
             dma((4,)),
             dma((4,)),
             dma,

time: 97.6 us -> 90.5 us (0.927)
  Pallas kernels: 95.6 us -> 88.5 us
    pallas_call x1, Pallas kernels: 95.6 us -> 88.5 us  [per_device(): pl.pallas_call(layer_kernel, out_shape=jax.ShapeDtypeStruct((OWN, D), BF1...]
where the time goes in v4:
time: 90.5 us; the launch traced here: 90.3 us
  Pallas kernels  88.5 us (98%)
  local copies, waits for them, and re-layouts  1.88 us (2%)
    pallas_call x1, Pallas kernels, per_device(): pl.pallas_call(layer_kernel, out_shape=jax.ShapeDtypeStruct((OWN, D), BF1...  88.5 us
    unnamed x1, local copies, waits for them, and re-layouts  1.88 us

profile of v4, /device:TPU:1, one launch (start us, length us, event | category | flops | bytes accessed | tf_op | source)
XLA Modules:
  0.0 90.3 jit_solution(15317373604560983665)
XLA Ops:
  0.0 88.5 %shard_map.199 = bf16[128,2048]{1,0:T(8,128)(2,1)} custom-call(bf16[128,2048]{1,0:T(8,128)(2,1)} %tok_hbm.1, bf16[2048]{0:T(1024)(128)(2,1)} %scale_hbm.1, bf16[16,256]{1,0:T(8,128)(2,1)} %outer_w.1, bf16[16,256]{1,0:T(8,128)(2,1)} %inner_w.1, bf16[16,256]{1,0:T(8,128)(2,1)} %value_w.1, bf16[16,256]{1,0:T(8,128)(2,1)} %out_gate_w.1, ...), custom_call_target="tpu_custom_call" | custom-call | tf_op jit(solution)/shard_map/pallas_call | solution.py:693
  88.5 1.9 %copy.23 = bf16[128,2048]{1,0:T(8,128)(2,1)} copy(bf16[128,2048]{1,0:T(8,128)(2,1)} %shard_map.199) | data formatting | bytes 1048576

commit v5 on v4

--- a/solution.py
+++ b/solution.py
@@ -24,7 +24,6 @@
 L = 128
 BLOCKS = LEN // L
 NA = 6
-HOP = 2
 GROUPS = 8
 OUTER, INNER, VALUE, CONV_T, STATE_T, OUT_GATE, STATE_IN, KEYS = range(8)
 EPS = 1e-05
@@ -177,7 +176,6 @@
 
     z_right, z_left = (zm(1), x, c, y), (zm(-1), x, c, y)
     x_right, x_left = (z, xm(1), c, y), (z, xm(-1), c, y)
-    z_far_right, z_far_left = (zm(HOP), x, c, y), (zm(-HOP), x, c, y)
     x_across = (z, xm(2), c, y)
     y_right, y_left = (z, x, c, ym(1)), (z, x, c, ym(-1))
     partner = (z, x, 1 - c, y)
@@ -236,7 +234,7 @@
     hello(along(-1))
 
     hello(partner)
-    for where in (z_right, z_left, z_far_right, z_far_left, x_right, x_left, x_across):
+    for where in (z_right, z_left, x_right, x_left, x_across):
         hello(where)
 
     def send(src, dst, s_sem, r_sem, where):
@@ -275,19 +273,16 @@
         return wbuf.at[zz, :, c, group]
 
     def goes_right(d):
-        return d != HOP - 1 and d < NZ // 2
+        return d < NZ // 2
 
     def goes_left(d):
-        return d != HOP - 1 and d < NZ // 2 - 1
+        return d < NZ // 2 - 1
 
     def z_pass(blk, k, s_sem, l_sem, r_sem, base):
         if k <= 0 and goes_right(-k):
             send(blk, blk, s_sem, l_sem.at[base - k], z_right)
         if k >= 0 and goes_left(k):
             send(blk, blk, s_sem, r_sem.at[base + k], z_left)
-        if k == 0:
-            send(blk, blk, s_sem, l_sem.at[base + HOP - 1], z_far_right)
-            send(blk, blk, s_sem, r_sem.at[base + HOP - 1], z_far_left)
 
     def z_wait(blk, k, l_sem, r_sem, base):
         wait(blk, l_sem.at[base - k - 1] if k < 0 else r_sem.at[base + k - 1])
@@ -332,13 +327,10 @@
     order_b = (KEYS, STATE_IN)
     LAST = -(NZ // 2)
     rounds = [((0,),)]
-    for r in range(1, max(HOP - 1, NZ // 2 - HOP + 1) + 1):
-        near = [(-r, r)] if r < HOP else []
-        d = r + HOP - 1
-        far = [(-d, d) if d < NZ // 2 else (-d,)] if d <= NZ // 2 else []
-        rounds.append(tuple(near + far))
-
-    pl.semaphore_wait(barrier, 11)
+    for r in range(1, 9):
+        rounds.append((((-r, r) if r < 8 else (-r,)),))
+
+    pl.semaphore_wait(barrier, 9)
     for copy in weight_copies:
         copy.wait()
     az_pass(0)

time: 90.5 us -> 90.2 us (level)
  no operation moved by 1% of the time
where the time goes in v5:
time: 90.2 us; the launch traced here: 90.1 us
  Pallas kernels  88.2 us (98%)
  local copies, waits for them, and re-layouts  1.88 us (2%)
    pallas_call x1, Pallas kernels, per_device(): pl.pallas_call(layer_kernel, out_shape=jax.ShapeDtypeStruct((OWN, D), BF1...  88.2 us
    unnamed x1, local copies, waits for them, and re-layouts  1.88 us

profile of v5, /device:TPU:1, one launch (start us, length us, event | category | flops | bytes accessed | tf_op | source)
XLA Modules:
  0.0 90.1 jit_solution(16368110610891252076)
XLA Ops:
  0.0 88.2 %shard_map.199 = bf16[128,2048]{1,0:T(8,128)(2,1)} custom-call(bf16[128,2048]{1,0:T(8,128)(2,1)} %tok_hbm.1, bf16[2048]{0:T(1024)(128)(2,1)} %scale_hbm.1, bf16[16,256]{1,0:T(8,128)(2,1)} %outer_w.1, bf16[16,256]{1,0:T(8,128)(2,1)} %inner_w.1, bf16[16,256]{1,0:T(8,128)(2,1)} %value_w.1, bf16[16,256]{1,0:T(8,128)(2,1)} %out_gate_w.1, ...), custom_call_target="tpu_custom_call" | custom-call | tf_op jit(solution)/shard_map/pallas_call | solution.py:685
  88.2 1.9 %copy.23 = bf16[128,2048]{1,0:T(8,128)(2,1)} copy(bf16[128,2048]{1,0:T(8,128)(2,1)} %shard_map.199) | data formatting | bytes 1048576
